TPU v7x, 32 devices: a whole 2x2x4 slice. The times are simulated.
32 devices in a mesh: sp: 8 (over z, y), tp: 4 (over x, core).
Axes of the slice: x: 2, y: 2, z: 4, core: 2. Of those that a mesh axis runs over, the one named last changes fastest.
Arguments:
- tokens: bfloat16 [2048, 4096], P('sp'), may hold values from -64 to 64
- norm_gain: float32 [4096], replicated, may hold values from 0.1 to 1.9
- w_query: bfloat16 [4096, 2048], P('sp', 'tp'), may hold values from -1.09375 to 1.09375
- w_key: bfloat16 [4096, 512], P('sp', 'tp'), may hold values from -0.09375 to 0.09375
- w_value: bfloat16 [4096, 512], P('sp', 'tp'), may hold values from -0.09375 to 0.09375
- w_glu: bfloat16 [4096, 2048], P('sp', 'tp'), may hold values from -0.09375 to 0.09375
- w_gate: bfloat16 [4096, 2048], P('sp', 'tp'), may hold values from -0.09375 to 0.09375
- sink_logit: float32 [32], P('tp'), may hold values from 2 to 6
- conv_taps: bfloat16 [31, 2048], P(None, 'tp'), may hold values from -12.9315817 to 12.9315817
- conv_gain: float32 [2048], P('tp'), may hold values from 0.1 to 1.9
- out_attn: bfloat16 [2048, 4096], P('sp', 'tp'), may hold values from -0.5 to 0.5
- out_conv: bfloat16 [2048, 4096], P('sp', 'tp'), may hold values from -0.125 to 0.125
Outputs:
- mixed: bfloat16 [2048, 4096], P('sp', 'tp')
All inputs are finite; a program needn't handle non-finite values.
Results may differ from a plain program's by a relative error of at most 0.008.
The roundings to bfloat16 on the way count: a program that leaves them out, or rounds other values in their place, can miss the bound.
Values may be sent and summed in bfloat16 or wider, within the bound.
A program may use at most 64 MiB of HBM per device.

v0:
```python
import functools
import math

import jax
import jax.numpy as jnp
from jax import lax
from jax.experimental import pallas as pl
from jax.experimental.pallas import tpu as pltpu
from jax.sharding import PartitionSpec as P

HEADS = 32
HEAD = 64
KV = 8
CONV = 2048
KSIZE = 31
WINDOW = 128


def passed_along(block, axis, distance):
    devices = range(lax.axis_size(axis))
    route = [(i - distance, i) for i in devices if i - distance in devices]
    return lax.ppermute(block, axis, route)


def rotate_heads(values, positions):
    half_width = values.shape[-1] // 2
    frequency = 10000.0 ** (-jnp.arange(half_width, dtype=jnp.float32) * 2.0 / values.shape[-1])
    angles = positions.astype(jnp.float32)[:, None] * frequency[None, :]
    cosine = jnp.cos(angles)[:, None, :]
    sine_part = jnp.sin(angles)[:, None, :]
    first_half = values[..., :half_width]
    second_half = values[..., half_width:]
    return jnp.concatenate(
        [
            first_half * cosine - second_half * sine_part,
            second_half * cosine + first_half * sine_part,
        ],
        axis=-1,
    )


def ring_gather_kernel(n, count, *refs):
    shards, wholes = refs[:count], refs[count : 2 * count]
    bounce = refs[2 * count : 3 * count]
    in_sem, out_sem, send_sem, recv_sem = refs[3 * count :]
    me = lax.axis_index("sp")
    half = n // 2
    odd = lax.rem(me, 2)
    place = (1 - odd) * lax.div(me, 2) + odd * (n - 1 - lax.div(me, 2))

    def device_at(position):
        spot = lax.rem(position + 2 * n, n)
        back = lax.div(spot, half)
        return (1 - back) * 2 * spot + back * (2 * (n - 1 - spot) + 1)

    ahead, behind = device_at(place + 1), device_at(place - 1)
    barrier = pltpu.get_barrier_semaphore()
    for neighbour in (ahead, behind):
        pl.semaphore_signal(
            barrier, inc=1, device_id={"sp": neighbour}, device_id_type=pl.DeviceIdType.MESH
        )
    pl.semaphore_wait(barrier, 2)

    def block(array, owner, way):
        rows = shards[array].shape[0]
        part = rows // 2
        start = pl.multiple_of(owner * rows + way * part, part)
        return wholes[array].at[pl.ds(start, part)]

    def hop(array, step, way):
        owner = device_at(place - step) if way == 0 else device_at(place + step)
        part = shards[array].shape[0] // 2
        target = block(array, owner, way)
        source = shards[array].at[pl.ds(way * part, part)] if step == 0 else target
        return pltpu.make_async_remote_copy(
            src_ref=source,
            dst_ref=target,
            send_sem=send_sem.at[way, step, array],
            recv_sem=recv_sem.at[way, step, array],
            device_id={"sp": ahead if way == 0 else behind},
            device_id_type=pl.DeviceIdType.MESH,
        )

    def arrival(array, step, way):
        owner = device_at(place - step - 1) if way == 0 else device_at(place + step + 1)
        target = block(array, owner, way)
        return pltpu.make_async_remote_copy(
            src_ref=target,
            dst_ref=target,
            send_sem=send_sem.at[way, step, array],
            recv_sem=recv_sem.at[way, step, array],
            device_id={"sp": ahead if way == 0 else behind},
            device_id_type=pl.DeviceIdType.MESH,
        )

    for array in range(count):
        for way in range(2):
            hop(array, 0, way).start()
    loads = [
        pltpu.make_async_copy(shards[a], bounce[a], in_sem.at[a]) for a in range(count)
    ]
    for load in loads:
        load.start()
    stores = []
    for a in range(count):
        loads[a].wait()
        rows = shards[a].shape[0]
        mine = wholes[a].at[pl.ds(pl.multiple_of(me * rows, rows), rows)]
        stores.append(pltpu.make_async_copy(bounce[a], mine, out_sem.at[a]))
        stores[a].start()
    for step in range(1, n - 1):
        for array in range(count):
            for way in range(2):
                arrival(array, step - 1, way).wait_recv()
                hop(array, step, way).start()
    for array in range(count):
        for way in range(2):
            arrival(array, n - 2, way).wait_recv()
    for step in range(n - 1):
        for array in range(count):
            for way in range(2):
                hop(array, step, way).wait_send()
    for store in stores:
        store.wait()


def ring_gather(arrays, collective_id):
    n = lax.axis_size("sp")
    count = len(arrays)
    return pl.pallas_call(
        functools.partial(ring_gather_kernel, n, count),
        out_shape=[
            jax.ShapeDtypeStruct((n * a.shape[0],) + a.shape[1:], a.dtype) for a in arrays
        ],
        in_specs=[pl.BlockSpec(memory_space=pl.ANY)] * count,
        out_specs=[pl.BlockSpec(memory_space=pl.ANY)] * count,
        scratch_shapes=[pltpu.VMEM(a.shape, a.dtype) for a in arrays]
        + [
            pltpu.SemaphoreType.DMA((count,)),
            pltpu.SemaphoreType.DMA((count,)),
            pltpu.SemaphoreType.DMA((2, n - 1, count)),
            pltpu.SemaphoreType.DMA((2, n - 1, count)),
        ],
        compiler_params=pltpu.CompilerParams(
            collective_id=collective_id, has_side_effects=True
        ),
    )(*arrays)


def per_device(
    tokens,
    norm_gain,
    w_query,
    w_key,
    w_value,
    w_glu,
    w_gate,
    sink_logit,
    conv_taps,
    conv_gain,
    out_attn,
    out_conv,
):
    row_count = tokens.shape[0]
    offset_rows = lax.axis_index("sp") * row_count
    positions = offset_rows + jnp.arange(row_count, dtype=jnp.int32)
    tokens_f = tokens.astype(jnp.float32)
    normed = (
        tokens_f
        * lax.rsqrt(jnp.mean(tokens_f * tokens_f, axis=1, keepdims=True) + 1e-06)
        * norm_gain
    ).astype(jnp.bfloat16)
    local_heads = w_query.shape[1] // HEAD
    local_kv = w_key.shape[1] // HEAD
    group_size = HEADS // KV
    kv_width = local_kv * HEAD
    *pieces, attn_rows, conv_rows = ring_gather(
        (w_query, w_key, w_value, w_glu, w_gate, out_attn, out_conv), 0
    )
    query_acc, key_acc, value_acc, glu_acc, gate_acc = tuple(
        (
            jnp.dot(normed, weight_piece, preferred_element_type=jnp.float32)
            for weight_piece in pieces
        )
    )
    queries = rotate_heads(query_acc.reshape(row_count, local_heads, HEAD), positions).astype(
        jnp.bfloat16
    )
    keys_rot = rotate_heads(key_acc.reshape(row_count, local_kv, HEAD), positions).astype(
        jnp.bfloat16
    )
    keys_rot = keys_rot.reshape(row_count, kv_width)
    values_bf = value_acc.astype(jnp.bfloat16)
    kv_tail = jnp.concatenate(
        [keys_rot[row_count - WINDOW :], values_bf[row_count - WINDOW :]], axis=1
    )
    kv_rim = passed_along(kv_tail, "sp", 1)
    gated = (glu_acc * jax.nn.sigmoid(gate_acc)).astype(jnp.bfloat16)
    conv_tail = gated[row_count - (KSIZE - 1) :]
    conv_rim = passed_along(conv_tail, "sp", 1)
    block_count = row_count // WINDOW
    keys_all = jnp.concatenate([kv_rim[:, :kv_width], keys_rot], axis=0).reshape(
        block_count + 1, WINDOW, local_kv, HEAD
    )
    vals_all = jnp.concatenate([kv_rim[:, kv_width:], values_bf], axis=0).reshape(
        block_count + 1, WINDOW, local_kv, HEAD
    )
    key_blocks = jnp.concatenate([keys_all[:-1], keys_all[1:]], axis=1)
    value_blocks = jnp.concatenate([vals_all[:-1], vals_all[1:]], axis=1)
    query_block_rows = queries.reshape(block_count, WINDOW, local_kv, group_size, HEAD)
    score_matrix = jnp.einsum(
        "bqhgd,bkhd->bhgqk", query_block_rows, key_blocks, preferred_element_type=jnp.float32
    ) * (1.0 / math.sqrt(HEAD))
    block_ids = jnp.arange(block_count, dtype=jnp.int32)[:, None, None]
    query_pos = (
        offset_rows + block_ids * WINDOW + jnp.arange(WINDOW, dtype=jnp.int32)[None, :, None]
    )
    key_pos = (
        offset_rows
        + (block_ids - 1) * WINDOW
        + jnp.arange(2 * WINDOW, dtype=jnp.int32)[None, None, :]
    )
    distance = query_pos - key_pos
    allowed = (distance >= 0) & (distance < WINDOW) & (key_pos >= 0)
    score_matrix = jnp.where(allowed[:, None, None], score_matrix, -1e30)
    sink_local = sink_logit.reshape(local_kv, group_size)[None, :, :, None, None]
    highest = jnp.maximum(jnp.max(score_matrix, axis=-1, keepdims=True), sink_local)
    weights_exp = jnp.exp(score_matrix - highest)
    denom_total = jnp.sum(weights_exp, axis=-1, keepdims=True) + jnp.exp(sink_local - highest)
    weights_bfloat_half = (weights_exp / denom_total).astype(jnp.bfloat16)
    attended_values = jnp.einsum(
        "bhgqk,bkhd->bqhgd", weights_bfloat_half, value_blocks, preferred_element_type=jnp.float32
    ).astype(jnp.bfloat16)
    attended_values = attended_values.reshape(row_count, local_heads * HEAD)
    extended = jnp.concatenate([conv_rim, gated], axis=0).astype(jnp.float32)
    filtered = lax.conv_general_dilated(
        extended[None],
        conv_taps.astype(jnp.float32)[:, None, :],
        (1,),
        "VALID",
        dimension_numbers=("NWC", "WIO", "NWC"),
        feature_group_count=extended.shape[1],
        precision=lax.Precision.HIGHEST,
    )[0]
    channel_sum, channel_square = lax.psum(
        (jnp.sum(filtered, axis=1), jnp.sum(filtered * filtered, axis=1)), "tp"
    )
    mean_value = channel_sum / CONV
    variance = channel_square / CONV - mean_value * mean_value
    scaled = (filtered - mean_value[:, None]) * lax.rsqrt(variance + 1e-05)[:, None] * conv_gain
    conv_out = jax.nn.silu(scaled).astype(jnp.bfloat16)
    pieces = (
        lax.all_gather(attended_values, "tp", axis=1, tiled=True),
        lax.all_gather(conv_out, "tp", axis=1, tiled=True),
    )
    mixed = jnp.dot(pieces[0], attn_rows, preferred_element_type=jnp.float32) + jnp.dot(
        pieces[1], conv_rows, preferred_element_type=jnp.float32
    )
    return mixed.astype(jnp.bfloat16)


def solution(mesh):
    return jax.shard_map(
        per_device,
        mesh=mesh,
        in_specs=(
            P("sp", None),
            P(),
            P("sp", "tp"),
            P("sp", "tp"),
            P("sp", "tp"),
            P("sp", "tp"),
            P("sp", "tp"),
            P("tp"),
            P(None, "tp"),
            P("tp"),
            P("sp", "tp"),
            P("sp", "tp"),
        ),
        out_specs=P("sp", "tp"),
        check_vma=False,
    )
```

profile of v0, /device:TPU:0, one launch (start us, length us, event | category | flops | bytes accessed | tf_op | source)
XLA Modules:
  0.0 298.9 jit_solution(12133648533888614277)
XLA Ops:
  6.6 2.2 fusion
  8.8 223.7 %shard_map.118 = (bf16[4096,512]{1,0:T(8,128)(2,1)}, bf16[4096,128]{1,0:T(8,128)(2,1)}, bf16[4096,128]{1,0:T(8,128)(2,1)}, bf16[4096,512]{1,0:T(8,128)(2,1)}, bf...) custom-call(bf16[512,512]{1,0:T(8,128)(2,1)} %refs_0_.1, ...), custom_call_target="tpu_custom_call" | custom-call | tf_op jit(solution)/shard_map/pallas_call | solution.py:130
  232.6 2.3 fusion.41
  234.9 0.8 convolution_convert_fusion.1
  235.7 0.2 multiply_cosine_fusion
  236.0 0.1 copy.24
  236.1 3.4 %collective-permute-start = (bf16[128,256]{1,0:T(8,128)(2,1)S(1)}, bf16[128,256]{1,0:T(8,128)(2,1)S(1)}, u32[]{:S(2)}, u32[]{:S(2)}) collective-permute-start(bf16[128,256]{1,0:T(8,128)(2,1)S(1)} %pad_maximum_fusion.2), channel_id=1, source_target_pairs={{0,4},{4,8},{8,12},{12,16},{16,20},{20,24},{24,28},{1,5},{5,9},{9,... | collective-permute-start | bytes 196616 | tf_op jit(solution)/shard_map/ppermute | solution.py:22
  239.6 0.1 broadcast_compare_fusion
  239.6 0.1 iota_add_fusion
  239.7 0.1 reshape.214
  239.8 0.1 max.18
  239.9 0.1 iota_add_fusion.1
  240.0 0.1 copy.28
  240.1 4.1 %fusion.38 = f32[256,512]{0,1:T(8,128)S(1)} fusion(bf16[4096,512]{1,0:T(8,128)(2,1)} %get-tuple-element.14, bf16[256,4096]{1,0:T(8,128)(2,1)S(1)} %copy-done.1, f32[4096]{0:T(1024)S(1)} %copy-done.4, f32[256]{0:T(256)S(1)} %add_rsqrt_fusion.1), kind=kOutput, calls=%fused_computation.80 | convolution fusion | flops 1077936128 | bytes 6833152 | tf_op jit(solution)/shard_map/dot_general | solution.py:182
  244.2 0.1 subtract_convert_fusion
  244.4 4.3 %fusion.7 = f32[256,512]{1,0:T(8,128)} fusion(bf16[4096,512]{1,0:T(8,128)(2,1)} %get-tuple-element.17, bf16[256,4096]{1,0:T(8,128)(2,1)S(1)} %copy-done.1, f32[4096]{0:T(1024)S(1)} %copy-done.4, f32[256]{0:T(256)S(1)} %add_rsqrt_fusion.1), kind=kOutput, calls=%fused_computation.15 | convolution fusion | flops 1078329344 | bytes 6833152 | tf_op jit(solution)/shard_map/dot_general | solution.py:182
  248.7 0.2 fusion.25
  249.0 0.1 copy.29
  249.2 0.1 reshape.213
  249.3 0.1 copy.27
  249.4 0.5 fusion.44
  249.9 0.1 broadcast_maximum_fusion
  250.0 0.3 fusion.3
  250.3 0.1 exponential_add_fusion
  250.4 0.5 fusion.9
  250.9 0.3 copy.36
  251.2 0.7 copy.55
  251.9 0.0 all-gather.3.cloned.1.call-update
  251.9 0.0 all-gather.5.cloned.1.call-start
  252.0 3.5 %fusion.8 = bf16[256,512]{1,0:T(8,128)(2,1)S(1)} fusion(f32[256,512]{1,0:T(8,128)S(1)} %copy-done.7, bf16[4096,512]{1,0:T(8,128)(2,1)} %get-tuple-element.16, bf16[256,4096]{1,0:T(8,128)(2,1)S(1)} %copy-done.1, f32[4096]{0:T(1024)S(1)} %copy-done.4, f32[256]{0:T(256)S(1)} %add_rsqrt_fusion.1), kind=kOutput, calls=%fused_computation.16 | convolution fusion | flops 1078198272 | bytes 7095296 | tf_op jit(solution)/shard_map/dot_general | solution.py:182
  255.5 3.6 %collective-permute-start.1 = (bf16[30,512]{1,0:T(8,128)(2,1)S(1)}, bf16[30,512]{1,0:T(8,128)(2,1)S(1)}, u32[]{:S(2)}, u32[]{:S(2)}) collective-permute-start(bf16[30,512]{1,0:T(8,128)(2,1)S(1)} %slice.73), channel_id=1, source_target_pairs={{0,4},{4,8},{8,12},{12,16},{16,20},{20,24},{24,28},{1,5},{5,9},{9,... | collective-permute-start | bytes 92168 | tf_op jit(solution)/shard_map/ppermute | solution.py:22
  259.1 1.4 collective-permute-done.1
  260.5 0.1 maximum_bitcast_fusion
  260.6 0.1 reshape.203
  260.7 0.1 copy.38
  260.8 0.1 slice.74
  260.9 1.4 convolution_select_fusion
  262.3 0.3 copy.40
  262.6 0.1 reshape.207
  262.7 0.1 slice_reduce_fusion
  262.8 0.1 fusion.19
  262.9 5.7 %all-reduce = (f32[256]{0:T(256)S(1)}, f32[256]{0:T(256)S(1)}) all-reduce(f32[256]{0:T(256)S(1)} %fusion.19, f32[256]{0:T(256)S(1)} %slice_reduce_fusion), channel_id=1, replica_groups=mesh['sp'=8,'tp'=4] {'tp'}, use_global_device_ids=true, to_apply=%region_6.7 | all-reduce | flops 512 | bytes 4096 | tf_op jit(solution)/shard_map/psum | solution.py:245
  268.6 1.0 multiply_convert_fusion
  269.5 0.0 all-gather.5.cloned.1.call-update
  269.6 0.0 all-gather.3.cloned.1.call-done
  269.6 3.8 %fusion.46 = f32[256,1024]{1,0:T(8,128)S(1)} fusion(bf16[256,2048]{0,1:T(8,128)(2,1)} %all-gather.3.cloned.1.call-done, bf16[2048,1024]{1,0:T(8,128)(2,1)} %get-tuple-element.15), kind=kOutput, calls=%fused_computation.85 | convolution fusion | flops 1073741824 | bytes 6291456 | tf_op jit(solution)/shard_map/dot_general | solution.py:256
  273.4 14.1 %all-gather.5.cloned.1.call-done = bf16[256,2048]{1,0:T(8,128)(2,1)} async-done(((bf16[256,512]{1,0:T(8,128)(2,1)}), bf16[256,2048]{1,0:T(8,128)(2,1)}) %all-gather.5.cloned.1.call-update) | async-done | bytes 1048592 | tf_op jit(solution)/shard_map/all_gather | solution.py:254
  287.5 4.6 %fusion.4 = bf16[256,1024]{1,0:T(8,128)(2,1)} fusion(f32[256,1024]{1,0:T(8,128)S(1)} %fusion.46, bf16[256,2048]{1,0:T(8,128)(2,1)} %all-gather.5.cloned.1.call-done, bf16[2048,1024]{1,0:T(8,128)(2,1)} %get-tuple-element.18), kind=kOutput, calls=%fused_computation.10 | convolution fusion | flops 1074266112 | bytes 6815744 | tf_op jit(solution)/shard_map/dot_general | solution.py:256
  (40 shorter events, 0.4 us)
Async XLA Ops:
  6.5 254.3 %copy-start = (bf16[31,512]{1,0:T(8,128)(2,1)S(1)}, bf16[31,512]{1,0:T(8,128)(2,1)}, u32[]{:S(2)}) copy-start(bf16[31,512]{1,0:T(8,128)(2,1)} %param.20) | copy-start | bytes 95236
  6.5 226.0 %copy-start.1 = (bf16[256,4096]{1,0:T(8,128)(2,1)S(1)}, bf16[256,4096]{1,0:T(8,128)(2,1)}, u32[]{:S(2)}) copy-start(bf16[256,4096]{1,0:T(8,128)(2,1)} %param.12) | copy-start | bytes 6291460
  6.5 226.0 %copy-start.4 = (f32[4096]{0:T(1024)S(1)}, f32[4096]{0:T(1024)}, u32[]{:S(2)}) copy-start(f32[4096]{0:T(1024)} %param.13) | copy-start | bytes 49156
  6.5 263.0 %all-gather.3.cloned.1.call-start = ((), (), s32[]{:S(2)}) async-start(), calls=%async_computation | async-start | bytes 1310720 | tf_op jit(solution)/shard_map/all_gather | solution.py:253
  232.5 2.3 copy-start.3
  232.6 7.2 %copy-start.5 = (f32[8]{0:T(128)S(1)}, f32[8]{0:T(128)}, u32[]{:S(2)}) copy-start(f32[8]{0:T(128)} %param.19) | copy-start | bytes 100
  236.1 12.8 %collective-permute-start = (bf16[128,256]{1,0:T(8,128)(2,1)S(1)}, bf16[128,256]{1,0:T(8,128)(2,1)S(1)}, u32[]{:S(2)}, u32[]{:S(2)}) collective-permute-start(bf16[128,256]{1,0:T(8,128)(2,1)S(1)} %pad_maximum_fusion.2), channel_id=1, source_target_pairs={{0,4},{4,8},{8,12},{12,16},{16,20},{20,24},{24,28},{1,5},{5,9},{9,... | collective-permute-start | bytes 196616 | tf_op jit(solution)/shard_map/ppermute | solution.py:22
  250.4 1.6 copy-start.7
  251.9 35.6 %all-gather.5.cloned.1.call-start = ((), (), s32[]{:S(2)}) async-start(), calls=%async_computation.1 | async-start | bytes 1310720 | tf_op jit(solution)/shard_map/all_gather | solution.py:254
  252.0 8.9 %copy-start.6 = (pred[8,36]{0,1:T(8,128)(4,1)S(1)}, pred[8,36]{0,1:T(8,128)(4,1)}, u32[]{:S(2)}) copy-start(pred[8,36]{0,1:T(8,128)(4,1)} %constant.53) | copy-start | bytes 868
  255.5 5.0 %collective-permute-start.1 = (bf16[30,512]{1,0:T(8,128)(2,1)S(1)}, bf16[30,512]{1,0:T(8,128)(2,1)S(1)}, u32[]{:S(2)}, u32[]{:S(2)}) collective-permute-start(bf16[30,512]{1,0:T(8,128)(2,1)S(1)} %slice.73), channel_id=1, source_target_pairs={{0,4},{4,8},{8,12},{12,16},{16,20},{20,24},{24,28},{1,5},{5,9},{9,... | collective-permute-start | bytes 92168 | tf_op jit(solution)/shard_map/ppermute | solution.py:22
  260.9 7.7 %copy-start.2 = (f32[512]{0:T(512)S(1)}, f32[512]{0:T(512)}, u32[]{:S(2)}) copy-start(f32[512]{0:T(512)} %param.21) | copy-start | bytes 6148
Sparse Core Ops, SparseCore 0:
  252.0 15.8 all-gather.2
  269.7 17.7 all-gather.4
where the time goes:
time: 299 us
  Pallas kernels  224 us (75%)
  matrix products  25.7 us (9%)
  waiting for transfers between devices  15.6 us (5%)
  between operations  13.8 us (5%)
  starting transfers between devices  7.09 us (2%)
  blocking collectives  5.67 us (2%)
  other arithmetic  4.76 us (2%)
    pallas_call x1, Pallas kernels, ring_gather(): pl.pallas_call(functools.partial(ring_gather_kernel, n, count), out_shape...  224 us
    dot_general x5, matrix products, per_device(): jnp.dot(normed, weight_piece, preferred_element_type=jnp.float32)  15 us
    all_gather x1, waiting for transfers between devices, per_device(): lax.all_gather(conv_out, 'tp', axis=1, tiled=True)  14.1 us
    ppermute x2, starting transfers between devices, passed_along(): return lax.ppermute(block, axis, route)  7.05 us
  transfers between devices with their start and end apart: 4, of which 2 were waited for; matrix products, arithmetic and copies ran while one was open for 7% of the time, Pallas kernels for 0%

commit v1 on v0

--- a/solution.py
+++ b/solution.py
@@ -147,7 +147,7 @@
     )(*arrays)
 
 
-def per_device(
+def gathered_per_device(
     tokens,
     norm_gain,
     w_query,
@@ -259,9 +259,824 @@
     return mixed.astype(jnp.bfloat16)
 
 
+MESH = pl.DeviceIdType.MESH
+A_CHUNKS = 2
+
+
+def remote(src, dst, sems, index, target, send_index=None):
+    send_sem, recv_sem = sems
+    return pltpu.make_async_remote_copy(
+        src_ref=src,
+        dst_ref=dst,
+        send_sem=send_sem.at[index if send_index is None else send_index],
+        recv_sem=recv_sem.at[index],
+        device_id=target,
+        device_id_type=MESH,
+    )
+
+
+def greet(targets):
+    barrier = pltpu.get_barrier_semaphore()
+    for target in targets:
+        pl.semaphore_signal(barrier, inc=1, device_id=target, device_id_type=MESH)
+    pl.semaphore_wait(barrier, len(targets))
+
+
+def spread_kernel(
+    planes,
+    normed,
+    w_query,
+    w_glu,
+    w_gate,
+    w_kv,
+    out_attn,
+    out_conv,
+    rows_all,
+    w_all,
+    out_other,
+    stage,
+    bounce,
+    local_sem,
+    a_send,
+    a_recv,
+    ax_send,
+    ax_recv,
+    ac_send,
+    ac_recv,
+    w1_send,
+    w1_recv,
+    w2_send,
+    w2_recv,
+    w3_send,
+    w3_recv,
+    kc_send,
+    kc_recv,
+    o_send,
+    o_recv,
+):
+    s, t = lax.axis_index("sp"), lax.axis_index("tp")
+    z, y, x, c = s // 2, s % 2, t // 2, t % 2
+    block = normed.shape[0]
+    piece = block // planes
+    step = piece // A_CHUNKS
+    depth = w_query.shape[0]
+    width = w_query.shape[1] // planes
+    three = 3 * width
+    half = depth // 2
+
+    def at(zz, yy, tt):
+        return {"sp": zz * 2 + yy, "tp": tt}
+
+    across_y = at(z, 1 - y, t)
+    across_x = at(z, y, (1 - x) * 2 + c)
+    diagonal = at(z, y, (1 - x) * 2 + (1 - c))
+    partner = at(z, y, x * 2 + (1 - c))
+    others = [lax.rem(z + k, planes) for k in range(1, planes)]
+    greet([across_y, across_x, diagonal, partner] + [at(zz, y, t) for zz in others])
+
+    def rows_of(zz, tt, chunk):
+        start = pl.multiple_of(zz * block + tt * piece + chunk * step, step)
+        return rows_all.at[pl.ds(start, step)]
+
+    def chain(way, distance, chunk):
+        from_z = z - distance if way == 0 else z + distance
+        to_z = z + 1 if way == 0 else z - 1
+        target = rows_of(from_z, t, chunk)
+        if distance == 0:
+            start = pl.multiple_of(t * piece + chunk * step, step)
+            source = normed.at[pl.ds(start, step)]
+        else:
+            source = target
+        index = (way * planes + distance) * A_CHUNKS + chunk
+        return remote(source, target, (a_send, a_recv), index, at(to_z, y, t))
+
+    def chain_arrival(way, distance, chunk):
+        from_z = z - distance if way == 0 else z + distance
+        index = (way * planes + distance - 1) * A_CHUNKS + chunk
+        return remote(rows_of(from_z, t, chunk), rows_of(from_z, t, chunk), (a_send, a_recv), index, across_x)
+
+    def can_send(way, distance):
+        if way == 0:
+            return jnp.logical_and(z - distance >= 0, z + 1 < planes)
+        return jnp.logical_and(z + distance < planes, z - 1 >= 0)
+
+    def exists(way, distance):
+        return z - distance >= 0 if way == 0 else z + distance < planes
+
+    def sideways(way, distance, chunk):
+        from_z = z - distance if way == 0 else z + distance
+        ref = rows_of(from_z, t, chunk)
+        index = (way * planes + distance) * A_CHUNKS + chunk
+        return remote(ref, ref, (ax_send, ax_recv), index, across_x)
+
+    def sideways_arrival(way, distance, chunk):
+        from_z = z - distance if way == 0 else z + distance
+        ref = rows_of(from_z, (1 - x) * 2 + c, chunk)
+        index = (way * planes + distance) * A_CHUNKS + chunk
+        return remote(ref, ref, (ax_send, ax_recv), index, across_x)
+
+    def to_partner(way, distance, chunk, far):
+        from_z = z - distance if way == 0 else z + distance
+        tt = (1 - x) * 2 + c if far else t
+        ref = rows_of(from_z, tt, chunk)
+        index = ((way * planes + distance) * A_CHUNKS + chunk) * 2 + far
+        return remote(ref, ref, (ac_send, ac_recv), index, partner)
+
+    def partner_arrival(way, distance, chunk, far):
+        from_z = z - distance if way == 0 else z + distance
+        tt = (1 - x) * 2 + (1 - c) if far else x * 2 + (1 - c)
+        ref = rows_of(from_z, tt, chunk)
+        index = ((way * planes + distance) * A_CHUNKS + chunk) * 2 + far
+        return remote(ref, ref, (ac_send, ac_recv), index, partner)
+
+    def home(zz, yy):
+        return pl.multiple_of((zz * 2 + yy) * depth, depth)
+
+    def wide(ref, start):
+        return ref.at[pl.ds(start, depth), pl.ds(0, three)]
+
+    def narrow(ref, start, cc):
+        return ref.at[pl.ds(pl.multiple_of(start + cc * half, half), half), pl.ds(three, width)]
+
+    def w_sources(tt):
+        cols = pl.ds(pl.multiple_of(tt * width, width), width)
+        return [w_query.at[:, cols], w_glu.at[:, cols], w_gate.at[:, cols], w_kv.at[tt]]
+
+    def w_targets(ref, start, cc):
+        rows = pl.ds(start, depth)
+        return [ref.at[rows, pl.ds(g * width, width)] for g in range(3)] + [narrow(ref, start, cc)]
+
+    def first(kind, target, tt, src_t, ref, start):
+        return [
+            remote(a, b, (w1_send, w1_recv), kind * 4 + i, target)
+            for i, (a, b) in enumerate(zip(w_sources(tt), w_targets(ref, start, tt % 2)))
+        ]
+
+    def first_all(kind, target, tt, what):
+        @pl.when(t == z)
+        def _():
+            for copy in first(kind, target, tt, t, w_all, home(z, y)):
+                what(copy)
+
+        @pl.when(t != z)
+        def _():
+            for copy in first(kind, target, tt, t, stage, pl.multiple_of(t * depth, depth)):
+                what(copy)
+
+    def first_arrival(kind, src_t):
+        @pl.when(src_t == z)
+        def _():
+            for i, ref in enumerate(w_targets(w_all, home(z, y), c)):
+                remote(ref, ref, (w1_send, w1_recv), kind * 4 + i, across_x).wait_recv()
+
+        @pl.when(src_t != z)
+        def _():
+            for i, ref in enumerate(w_targets(stage, pl.multiple_of(src_t * depth, depth), c)):
+                remote(ref, ref, (w1_send, w1_recv), kind * 4 + i, across_x).wait_recv()
+
+    def second_local():
+        return [
+            remote(a, b, (w2_send, w2_recv), z * 4 + i, at(t, y, t), t * 4 + i)
+            for i, (a, b) in enumerate(zip(w_sources(t), w_targets(w_all, home(z, y), c)))
+        ]
+
+    def second_staged(src_t):
+        start = pl.multiple_of(src_t * depth, depth)
+        return [
+            remote(a, b, (w2_send, w2_recv), z * 4 + i, at(src_t, y, t), src_t * 4 + i)
+            for a, b, i in (
+                (wide(stage, start), wide(w_all, home(z, y)), 0),
+                (narrow(stage, start, c), narrow(w_all, home(z, y), c), 3),
+            )
+        ]
+
+    def second_arrival(from_z):
+        ref_start = home(from_z, y)
+
+        @pl.when(t == z)
+        def _():
+            for i, ref in enumerate(w_targets(w_all, ref_start, c)):
+                remote(ref, ref, (w2_send, w2_recv), from_z * 4 + i, across_x).wait_recv()
+
+        @pl.when(t != z)
+        def _():
+            for ref, index in (
+                (wide(w_all, ref_start), from_z * 4),
+                (narrow(w_all, ref_start, c), from_z * 4 + 3),
+            ):
+                remote(ref, ref, (w2_send, w2_recv), index, across_x).wait_recv()
+
+    def third(from_z):
+        start = home(from_z, y)
+        return [
+            remote(wide(w_all, start), wide(w_all, start), (w3_send, w3_recv), from_z * 2, across_y),
+            remote(narrow(w_all, start, c), narrow(w_all, start, c), (w3_send, w3_recv), from_z * 2 + 1, across_y),
+        ]
+
+    def third_arrival(from_z):
+        start = home(from_z, 1 - y)
+        for ref, index in (
+            (narrow(w_all, start, c), from_z * 2 + 1),
+            (wide(w_all, start), from_z * 2),
+        ):
+            remote(ref, ref, (w3_send, w3_recv), index, across_y).wait_recv()
+
+    def to_share(from_z, own):
+        ref = narrow(w_all, home(from_z, y if own else 1 - y), c)
+        return remote(ref, ref, (kc_send, kc_recv), from_z * 2 + own, partner)
+
+    def share_arrival(from_z, own):
+        ref = narrow(w_all, home(from_z, y if own else 1 - y), 1 - c)
+        return remote(ref, ref, (kc_send, kc_recv), from_z * 2 + own, partner)
+
+    outs = [
+        remote(out_attn, out_other.at[0], (o_send, o_recv), 0, across_y),
+        remote(out_conv, out_other.at[1], (o_send, o_recv), 1, across_y),
+    ]
+
+    own_rows = pltpu.make_async_copy(
+        normed, rows_all.at[pl.ds(pl.multiple_of(z * block, block), block)], local_sem.at[0]
+    )
+    own_rows.start()
+
+    for chunk in range(A_CHUNKS):
+        for way in range(2):
+            @pl.when(can_send(way, 0))
+            def _():
+                chain(way, 0, chunk).start()
+    tx, td, tp = (1 - x) * 2 + c, (1 - x) * 2 + (1 - c), x * 2 + (1 - c)
+    first_all(2, partner, tp, lambda copy: copy.start())
+    first_all(0, across_x, tx, lambda copy: copy.start())
+    first_all(1, diagonal, td, lambda copy: copy.start())
+    for copy in outs:
+        copy.start()
+
+    @pl.when(t != z)
+    def _():
+        for copy in second_local():
+            copy.start()
+
+    def loads():
+        return [
+            pltpu.make_async_copy(a, b, local_sem.at[1 + i])
+            for i, (a, b) in enumerate(zip(w_sources(t), [bounce.at[:, pl.ds(g * width, width)] for g in range(3)] + [bounce.at[pl.ds(0, half), pl.ds(three, width)]]))
+        ]
+
+    def stores():
+        return [
+            pltpu.make_async_copy(a, b, local_sem.at[1 + i])
+            for i, (a, b) in enumerate(zip([bounce.at[:, pl.ds(g * width, width)] for g in range(3)] + [bounce.at[pl.ds(0, half), pl.ds(three, width)]], w_targets(w_all, home(z, y), c)))
+        ]
+
+    @pl.when(t == z)
+    def _():
+        for copy in loads():
+            copy.start()
+        for copy in loads():
+            copy.wait()
+        for copy in stores():
+            copy.start()
+        for copy in stores():
+            copy.wait()
+
+    def pass_on(src_t):
+        @pl.when(src_t != z)
+        def _():
+            for copy in second_staged(src_t):
+                copy.start()
+
+    def chain_step(distance):
+        for chunk in range(A_CHUNKS):
+            for way in range(2):
+                @pl.when(exists(way, distance))
+                def _():
+                    chain_arrival(way, distance, chunk).wait_recv()
+
+                    @pl.when(can_send(way, distance))
+                    def _():
+                        chain(way, distance, chunk).start()
+
+                    sideways(way, distance, chunk).start()
+                    to_partner(way, distance, chunk, 0).start()
+
+    def sideways_step(distance):
+        for chunk in range(A_CHUNKS):
+            for way in range(2):
+                @pl.when(exists(way, distance))
+                def _():
+                    sideways_arrival(way, distance, chunk).wait_recv()
+                    to_partner(way, distance, chunk, 1).start()
+
+    def settle(from_z):
+        for copy in third(from_z):
+            copy.start()
+        to_share(from_z, 1).start()
+
+    first_arrival(2, tp)
+    pass_on(tp)
+    chain_step(1)
+    first_arrival(0, tx)
+    pass_on(tx)
+    first_arrival(1, td)
+    pass_on(td)
+    settle(z)
+
+    def plane_step(distance):
+        for way in range(2):
+            from_z = z - distance if way == 0 else z + distance
+
+            @pl.when(exists(way, distance))
+            def _():
+                second_arrival(from_z)
+                settle(from_z)
+
+    plane_step(1)
+    chain_step(2)
+    sideways_step(1)
+    plane_step(2)
+    chain_step(3)
+    plane_step(3)
+    sideways_step(2)
+    sideways_step(3)
+    for k in range(planes):
+        from_z = lax.rem(z + k, planes)
+        third_arrival(from_z)
+        to_share(from_z, 0).start()
+    for copy in outs:
+        copy.wait_recv()
+    for distance in range(1, planes):
+        for chunk in range(A_CHUNKS):
+            for way in range(2):
+                @pl.when(exists(way, distance))
+                def _():
+                    for far in range(2):
+                        partner_arrival(way, distance, chunk, far).wait_recv()
+    for k in range(planes):
+        from_z = lax.rem(z + k, planes)
+        for own in range(2):
+            share_arrival(from_z, own).wait_recv()
+
+    own_rows.wait()
+    for copy in outs:
+        copy.wait_send()
+    first_all(2, partner, tp, lambda copy: copy.wait_send())
+    first_all(0, across_x, tx, lambda copy: copy.wait_send())
+    first_all(1, diagonal, td, lambda copy: copy.wait_send())
+
+    @pl.when(t != z)
+    def _():
+        for copy in second_local():
+            copy.wait_send()
+
+    for src_t in (tp, tx, td):
+        @pl.when(src_t != z)
+        def _():
+            for copy in second_staged(src_t):
+                copy.wait_send()
+
+    for k in range(planes):
+        from_z = lax.rem(z + k, planes)
+        for copy in third(from_z):
+            copy.wait_send()
+        for own in range(2):
+            to_share(from_z, own).wait_send()
+    for distance in range(planes):
+        for chunk in range(A_CHUNKS):
+            for way in range(2):
+                @pl.when(can_send(way, distance))
+                def _():
+                    chain(way, distance, chunk).wait_send()
+
+                if distance:
+                    @pl.when(exists(way, distance))
+                    def _():
+                        sideways(way, distance, chunk).wait_send()
+                        for far in range(2):
+                            to_partner(way, distance, chunk, far).wait_send()
+
+
+def spread(normed, w_query, w_glu, w_gate, w_kv, out_attn, out_conv, planes):
+    depth, cols = w_query.shape
+    width = cols // planes
+    any_spec = pl.BlockSpec(memory_space=pl.ANY)
+    count = 2 * planes * A_CHUNKS
+    pairs = [count, count, 2 * count, 12, 4 * planes, 2 * planes, 2 * planes, 2]
+    sems = []
+    for n in pairs:
+        sems += [pltpu.SemaphoreType.DMA((n,)), pltpu.SemaphoreType.DMA((n,))]
+    return pl.pallas_call(
+        functools.partial(spread_kernel, planes),
+        out_shape=[
+            jax.ShapeDtypeStruct((planes * normed.shape[0], normed.shape[1]), jnp.bfloat16),
+            jax.ShapeDtypeStruct((2 * planes * depth, 4 * width), jnp.bfloat16),
+            jax.ShapeDtypeStruct((2,) + out_attn.shape, jnp.bfloat16),
+            jax.ShapeDtypeStruct((planes * depth, 4 * width), jnp.bfloat16),
+        ],
+        in_specs=[pl.BlockSpec(memory_space=pltpu.VMEM)] + [any_spec] * 6,
+        out_specs=[any_spec] * 4,
+        scratch_shapes=[
+            pltpu.VMEM((depth, 4 * width), jnp.bfloat16),
+            pltpu.SemaphoreType.DMA((8,)),
+        ]
+        + sems,
+        compiler_params=pltpu.CompilerParams(collective_id=0, has_side_effects=True),
+    )(normed, w_query, w_glu, w_gate, w_kv, out_attn, out_conv)
+
+
+OUT_CHUNKS = 2
+
+
+def merge_kernel(
+    planes,
+    channels,
+    att,
+    filtered,
+    stats,
+    gain,
+    out_attn,
+    out_conv,
+    out_other,
+    mixed,
+    act,
+    weights,
+    stats_all,
+    in_up,
+    in_down,
+    outgoing,
+    local_sem,
+    s_send,
+    s_recv,
+    x_send,
+    x_recv,
+    c_send,
+    c_recv,
+    r_send,
+    r_recv,
+):
+    s, t = lax.axis_index("sp"), lax.axis_index("tp")
+    z, y, x, c = s // 2, s % 2, t // 2, t % 2
+    width = att.shape[1]
+    rows = att.shape[0]
+    block = rows // planes
+    group = out_attn.shape[0]
+    part = planes * width
+
+    def at(zz, yy, tt):
+        return {"sp": zz * 2 + yy, "tp": tt}
+
+    size = planes * planes
+    mine = z * planes + t
+    peers = [lax.rem(mine + k, size) for k in range(1, size)]
+    greet([at(g // planes, y, g % planes) for g in peers])
+    tx, tp = (1 - x) * 2 + c, x * 2 + (1 - c)
+    td = (1 - x) * 2 + (1 - c)
+
+    loads = [
+        pltpu.make_async_copy(
+            a, weights.at[pl.ds(pl.multiple_of(base + yy * group, group), group)], local_sem.at[i]
+        )
+        for i, (a, base, yy) in enumerate(
+            (
+                (out_attn, 0, y),
+                (out_other.at[0], 0, 1 - y),
+                (out_conv, part, y),
+                (out_other.at[1], part, 1 - y),
+            )
+        )
+    ]
+    for load in loads:
+        load.start()
+
+    def stat(k):
+        g = peers[k]
+        return pltpu.make_async_remote_copy(
+            src_ref=stats,
+            dst_ref=stats_all.at[mine],
+            send_sem=s_send.at[k],
+            recv_sem=s_recv.at[mine],
+            device_id=at(g // planes, y, g % planes),
+            device_id_type=MESH,
+        )
+
+    for k in range(size - 1):
+        stat(k).start()
+
+    def columns(kind, tt):
+        return pl.ds(pl.multiple_of(kind * part + tt * width, width), width)
+
+    def region(kind, r, tt):
+        return act.at[pl.ds(r * block, block), columns(kind, tt)]
+
+    def source(kind, r):
+        return att.at[pl.ds(r * block, block)] if kind == 0 else region(1, r, t)
+
+    def cross(kind, r):
+        return remote(source(kind, r), region(kind, r, t), (x_send, x_recv), kind * planes + r, at(z, y, tx))
+
+    def cross_arrival(kind, r):
+        return remote(region(kind, r, tx), region(kind, r, tx), (x_send, x_recv), kind * planes + r, at(z, y, tx))
+
+    def hand(kind, r, far):
+        src = region(kind, r, tx) if far else source(kind, r)
+        dst = region(kind, r, tx) if far else region(kind, r, t)
+        return remote(src, dst, (c_send, c_recv), (kind * planes + r) * 2 + far, at(z, y, tp))
+
+    def hand_arrival(kind, r, far):
+        ref = region(kind, r, td if far else tp)
+        return remote(ref, ref, (c_send, c_recv), (kind * planes + r) * 2 + far, at(z, y, tp))
+
+    for r in range(planes):
+        cross(0, r).start()
+        hand(0, r, 0).start()
+    act[:, columns(0, t)] = att[...]
+    stats_all[mine] = stats[...]
+    for g in peers:
+        ref = stats_all.at[g]
+        pltpu.make_async_remote_copy(
+            src_ref=ref,
+            dst_ref=ref,
+            send_sem=s_send.at[0],
+            recv_sem=s_recv.at[g],
+            device_id=at(z, y, tp),
+            device_id_type=MESH,
+        ).wait_recv()
+    total = stats_all[0]
+    for g in range(1, size):
+        total = total + stats_all[g]
+    tiles = total.shape[0] // 2
+    mean = total[:tiles] / channels
+    variance = total[tiles:] / channels - mean * mean
+    rate = lax.rsqrt(variance + 1e-05)
+    lanes = total.shape[1]
+    per = block // lanes
+    for r in range(planes):
+        for k in range(r * per, (r + 1) * per):
+            mean_col = jnp.transpose(jnp.broadcast_to(mean[k : k + 1], (lanes, lanes)))
+            rate_col = jnp.transpose(jnp.broadcast_to(rate[k : k + 1], (lanes, lanes)))
+            scaled = (filtered[k * lanes : (k + 1) * lanes] - mean_col[:, :width]) * rate_col[:, :width] * gain[...]
+            act[k * lanes : (k + 1) * lanes, columns(1, t)] = (scaled / (1.0 + jnp.exp(-scaled))).astype(act.dtype)
+        cross(1, r).start()
+        hand(1, r, 0).start()
+    for kind in range(2):
+        for r in range(planes):
+            cross_arrival(kind, r).wait_recv()
+            hand(kind, r, 1).start()
+    for load in loads:
+        load.wait()
+    for kind in range(2):
+        for r in range(planes):
+            for far in range(2):
+                hand_arrival(kind, r, far).wait_recv()
+
+    step = block // OUT_CHUNKS
+
+    def partial(r, h, tile, wide):
+        start = pl.multiple_of(r * block + h * step, step)
+        cols = pl.ds(pl.multiple_of(tile * wide, wide), wide)
+        return jnp.dot(act[pl.ds(start, step), :], weights[:, cols], preferred_element_type=jnp.float32), cols
+
+    columns_out = mixed.shape[1]
+    wide = min(256, columns_out)
+    tiles_out = columns_out // wide
+
+    def travel(way, r, h):
+        rows_h = pl.ds(h * step, step)
+        index = (way * planes + r) * OUT_CHUNKS + h
+        into = in_up if way == 0 else in_down
+        return remote(
+            outgoing.at[r, rows_h],
+            into.at[r, rows_h],
+            (r_send, r_recv),
+            index,
+            at(z + 1 if way == 0 else z - 1, y, t),
+        )
+
+    def travelled(way, r, h):
+        rows_h = pl.ds(h * step, step)
+        index = (way * planes + r) * OUT_CHUNKS + h
+        into = (in_up if way == 0 else in_down).at[r, rows_h]
+        return remote(into, into, (r_send, r_recv), index, at(z, y, tp))
+
+    for distance in range(planes - 1, 0, -1):
+        for h in range(OUT_CHUNKS):
+            rows_h = pl.ds(h * step, step)
+            for way in range(2):
+                r = z + distance if way == 0 else z - distance
+                there = r < planes if way == 0 else r >= 0
+                more = z > 0 if way == 0 else z < planes - 1
+                into = in_up if way == 0 else in_down
+
+                @pl.when(jnp.logical_and(there, jnp.logical_not(more)))
+                def _():
+                    @pl.loop(0, tiles_out)
+                    def _(tile):
+                        value, cols = partial(r, h, tile, wide)
+                        outgoing[r, rows_h, cols] = value.astype(outgoing.dtype)
+
+                    travel(way, r, h).start()
+
+                @pl.when(jnp.logical_and(there, more))
+                def _():
+                    travelled(way, r, h).wait_recv()
+
+                    @pl.loop(0, tiles_out)
+                    def _(tile):
+                        value, cols = partial(r, h, tile, wide)
+                        outgoing[r, rows_h, cols] = (
+                            value + into[r, rows_h, cols].astype(jnp.float32)
+                        ).astype(outgoing.dtype)
+
+                    travel(way, r, h).start()
+
+    for h in range(OUT_CHUNKS):
+        rows_h = pl.ds(h * step, step)
+
+        @pl.when(z > 0)
+        def _():
+            travelled(0, z, h).wait_recv()
+
+        @pl.when(z < planes - 1)
+        def _():
+            travelled(1, z, h).wait_recv()
+
+        @pl.loop(0, tiles_out)
+        def _(tile):
+            value, cols = partial(z, h, tile, wide)
+            below = in_up[z, rows_h, cols].astype(jnp.float32)
+            above = in_down[z, rows_h, cols].astype(jnp.float32)
+            value = value + jnp.where(z > 0, below, 0.0) + jnp.where(z < planes - 1, above, 0.0)
+            mixed[rows_h, cols] = value.astype(mixed.dtype)
+
+    for k in range(size - 1):
+        stat(k).wait_send()
+    for kind in range(2):
+        for r in range(planes):
+            cross(kind, r).wait_send()
+            for far in range(2):
+                hand(kind, r, far).wait_send()
+    for distance in range(1, planes):
+        for h in range(OUT_CHUNKS):
+            for way in range(2):
+                r = z + distance if way == 0 else z - distance
+
+                @pl.when(r < planes if way == 0 else r >= 0)
+                def _():
+                    travel(way, r, h).wait_send()
+
+
+def merge(att, filtered, stats, gain, out_attn, out_conv, out_other, planes, channels):
+    rows, width = att.shape
+    block = rows // planes
+    any_spec = pl.BlockSpec(memory_space=pl.ANY)
+    vmem = pl.BlockSpec(memory_space=pltpu.VMEM)
+    cols = out_attn.shape[1]
+    size = planes * planes
+    dma = pltpu.SemaphoreType.DMA
+    return pl.pallas_call(
+        functools.partial(merge_kernel, planes, channels),
+        out_shape=jax.ShapeDtypeStruct((block, cols), jnp.bfloat16),
+        in_specs=[vmem] * 4 + [any_spec] * 3,
+        out_specs=vmem,
+        scratch_shapes=[
+            pltpu.VMEM((rows, 2 * planes * width), jnp.bfloat16),
+            pltpu.VMEM((2 * planes * width, cols), jnp.bfloat16),
+            pltpu.VMEM((size,) + stats.shape, jnp.float32),
+            pltpu.VMEM((planes, block, cols), jnp.bfloat16),
+            pltpu.VMEM((planes, block, cols), jnp.bfloat16),
+            pltpu.VMEM((planes, block, cols), jnp.bfloat16),
+            dma((4,)),
+            dma((size,)),
+            dma((size,)),
+            dma((2 * planes,)),
+            dma((2 * planes,)),
+            dma((4 * planes,)),
+            dma((4 * planes,)),
+            dma((2 * planes * OUT_CHUNKS,)),
+            dma((2 * planes * OUT_CHUNKS,)),
+        ],
+        compiler_params=pltpu.CompilerParams(collective_id=1, has_side_effects=True),
+    )(att, filtered, stats, gain, out_attn, out_conv, out_other)
+
+
+def spread_per_device(
+    tokens,
+    norm_gain,
+    w_query,
+    w_key,
+    w_value,
+    w_glu,
+    w_gate,
+    sink_logit,
+    conv_taps,
+    conv_gain,
+    out_attn,
+    out_conv,
+):
+    planes = lax.axis_size("tp")
+    block = tokens.shape[0]
+    rows = planes * block
+    s, t = lax.axis_index("sp"), lax.axis_index("tp")
+    z, y = s // 2, s % 2
+    tokens_f = tokens.astype(jnp.float32)
+    normed = (
+        tokens_f
+        * lax.rsqrt(jnp.mean(tokens_f * tokens_f, axis=1, keepdims=True) + 1e-06)
+        * norm_gain
+    ).astype(jnp.bfloat16)
+    depth = w_key.shape[0]
+    kv = jnp.concatenate(
+        [w_key.reshape(2, depth // 2, 2, HEAD), w_value.reshape(2, depth // 2, 2, HEAD)], axis=-1
+    )
+    w_kv = jnp.transpose(kv, (2, 0, 1, 3)).reshape(planes, depth // 2, 2 * HEAD)
+    rows_all, w_all, out_other, _ = spread(
+        normed, w_query, w_glu, w_gate, w_kv, out_attn, out_conv, planes
+    )
+    width = w_query.shape[1] // planes
+    heads = width // HEAD
+    acc = jnp.dot(rows_all, w_all, preferred_element_type=jnp.float32)
+    positions = (
+        (2 * jnp.arange(planes, dtype=jnp.int32) + y)[:, None] * block
+        + jnp.arange(block, dtype=jnp.int32)[None, :]
+    )
+    flat_positions = positions.reshape(rows)
+    queries = rotate_heads(acc[:, :width].reshape(rows, heads, HEAD), flat_positions).astype(
+        jnp.bfloat16
+    )
+    keys_rot = rotate_heads(
+        acc[:, 3 * width : 3 * width + HEAD].reshape(rows, 1, HEAD), flat_positions
+    ).astype(jnp.bfloat16)
+    keys_rot = keys_rot.reshape(planes, block, HEAD)
+    values_bf = acc[:, 3 * width + HEAD :].astype(jnp.bfloat16).reshape(planes, block, HEAD)
+    gated = (acc[:, width : 2 * width] * jax.nn.sigmoid(acc[:, 2 * width : 3 * width])).astype(
+        jnp.bfloat16
+    )
+    gated = gated.reshape(planes, block, width)
+    kv_tail = jnp.concatenate([keys_rot, values_bf], axis=2)[:, block - WINDOW :]
+    tails = jnp.concatenate([kv_tail, gated[:, block - (KSIZE - 1) :]], axis=1)
+    flips = [(i, i ^ 1) for i in range(lax.axis_size("sp"))]
+    came = lax.ppermute(tails, "sp", flips)
+    earlier = jnp.concatenate([jnp.zeros_like(came[:1]), came[:-1]], axis=0)
+    rim = jnp.where(y == 1, came, earlier)
+    blocks = block // WINDOW
+    keys_all = jnp.concatenate([rim[:, :WINDOW, :HEAD], keys_rot], axis=1).reshape(
+        planes, blocks + 1, WINDOW, HEAD
+    )
+    vals_all = jnp.concatenate([rim[:, :WINDOW, HEAD:], values_bf], axis=1).reshape(
+        planes, blocks + 1, WINDOW, HEAD
+    )
+    key_blocks = jnp.concatenate([keys_all[:, :-1], keys_all[:, 1:]], axis=2).reshape(
+        planes * blocks, 2 * WINDOW, HEAD
+    )
+    value_blocks = jnp.concatenate([vals_all[:, :-1], vals_all[:, 1:]], axis=2).reshape(
+        planes * blocks, 2 * WINDOW, HEAD
+    )
+    query_blocks = queries.reshape(planes * blocks, WINDOW, heads, HEAD)
+    scores = jnp.einsum(
+        "bqgd,bkd->bgqk", query_blocks, key_blocks, preferred_element_type=jnp.float32
+    ) * (1.0 / math.sqrt(HEAD))
+    starts = positions[:, ::WINDOW].reshape(planes * blocks)[:, None, None]
+    query_pos = starts + jnp.arange(WINDOW, dtype=jnp.int32)[None, :, None]
+    key_pos = starts - WINDOW + jnp.arange(2 * WINDOW, dtype=jnp.int32)[None, None, :]
+    distance = query_pos - key_pos
+    allowed = (distance >= 0) & (distance < WINDOW) & (key_pos >= 0)
+    scores = jnp.where(allowed[:, None], scores, -1e30)
+    sink_all = lax.all_gather(sink_logit, "tp", tiled=True)
+    sinks = lax.dynamic_slice(sink_all, (z * planes * heads + t * heads,), (heads,))
+    sinks = sinks[None, :, None, None]
+    highest = jnp.maximum(jnp.max(scores, axis=-1, keepdims=True), sinks)
+    weights_exp = jnp.exp(scores - highest)
+    denom = jnp.sum(weights_exp, axis=-1, keepdims=True) + jnp.exp(sinks - highest)
+    probs = (weights_exp / denom).astype(jnp.bfloat16)
+    attended = jnp.einsum(
+        "bgqk,bkd->bqgd", probs, value_blocks, preferred_element_type=jnp.float32
+    ).astype(jnp.bfloat16)
+    attended = attended.reshape(rows, width)
+    extended = jnp.concatenate([rim[:, WINDOW:], gated], axis=1).astype(jnp.float32)
+    small = jnp.concatenate([conv_taps.astype(jnp.float32), conv_gain[None]], axis=0)
+    small = lax.all_gather(small, "tp", axis=1, tiled=True)
+    small = lax.dynamic_slice(small, (0, (z * planes + t) * width), (KSIZE + 1, width))
+    filtered = lax.conv_general_dilated(
+        extended,
+        small[:KSIZE, None, :],
+        (1,),
+        "VALID",
+        dimension_numbers=("NWC", "WIO", "NWC"),
+        feature_group_count=width,
+        precision=lax.Precision.HIGHEST,
+    ).reshape(rows, width)
+    stats = jnp.concatenate(
+        [jnp.sum(filtered, axis=1).reshape(-1, 128), jnp.sum(filtered * filtered, axis=1).reshape(-1, 128)]
+    )
+    return merge(
+        attended, filtered, stats, small[KSIZE:], out_attn, out_conv, out_other, planes, CONV
+    )
+
+
 def solution(mesh):
+    planes, others = mesh.shape["tp"], mesh.shape["sp"]
+    fits = others == 2 * planes and planes % 2 == 0 and HEADS % (planes * planes) == 0
     return jax.shard_map(
-        per_device,
+        spread_per_device if fits else gathered_per_device,
         mesh=mesh,
         in_specs=(
             P("sp", None),

time: 299 us -> 198 us (0.66)
  Pallas kernels: 224 us -> 154 us
  waiting for transfers between devices: 15.6 us -> 0.01 us
  matrix products: 25.7 us -> 11.5 us
  between operations: 13.8 us -> 1.12 us
  local copies, waits for them, and re-layouts: 2.56 us -> 10.3 us
  starting transfers between devices: 7.09 us -> 0.57 us
  blocking collectives: 5.67 us -> 11.8 us
  other arithmetic: 4.76 us -> 9.11 us
    pallas_call x1 -> x2, Pallas kernels: 224 us -> 154 us  [the longest x1 91.6 us: spread(): pl.pallas_call(functools.partial(spread_kernel, planes), out_shape=[jax.S...]
    dot_general x9 -> x3, matrix products: 24.3 us -> 9.28 us  [the longest x1 8.25 us: spread_per_device(): acc = jnp.dot(rows_all, w_all, preferred_element_type=jnp.float32)]
    all_gather x2 -> x0, waiting for transfers between devices: 14.2 us -> none  [the longest x1 14.1 us: per_device(): lax.all_gather(conv_out, 'tp', axis=1, tiled=True)]
    ppermute x2 -> x1, starting transfers between devices: 7.05 us -> 0.57 us  [spread_per_device(): came = lax.ppermute(tails, 'sp', flips)]
    all_gather x0 -> x1, blocking collectives: none -> 6.06 us  [spread_per_device(): small = lax.all_gather(small, 'tp', axis=1, tiled=True)]
    unnamed x0 -> x1, blocking collectives: none -> 5.78 us
    psum x1 -> x0, blocking collectives: 5.67 us -> none  [per_device(): lax.psum((jnp.sum(filtered, axis=1), jnp.sum(filtered * filtered, axis=1)...]
    unnamed x17 -> x23, local copies, waits for them, and re-layouts: 0.78 us -> 3.86 us
  transfers between devices with their start and end apart: 4 -> 1, of which waited for: 2 -> 0; matrix products, arithmetic and copies ran while one was open for 7% -> 2% of each run, Pallas kernels for 0% -> 0%
where the time goes in v1:
time: 198 us
  Pallas kernels  154 us (78%)
  blocking collectives  11.8 us (6%)
  matrix products  11.5 us (6%)
  local copies, waits for them, and re-layouts  10.3 us (5%)
  other arithmetic  9.11 us (5%)
    pallas_call x1, Pallas kernels, spread(): pl.pallas_call(functools.partial(spread_kernel, planes), out_shape=[jax.S...  91.6 us
    pallas_call x1, Pallas kernels, merge(): pl.pallas_call(functools.partial(merge_kernel, planes, channels), out_sha...  62.1 us
    dot_general x1, matrix products, spread_per_device(): acc = jnp.dot(rows_all, w_all, preferred_element_type=jnp.float32)  8.25 us
    all_gather x1, blocking collectives, spread_per_device(): small = lax.all_gather(small, 'tp', axis=1, tiled=True)  6.06 us
    unnamed x1, blocking collectives  5.78 us
  transfers between devices with their start and end apart: 1, of which 0 were waited for; matrix products, arithmetic and copies ran while one was open for 2% of the time, Pallas kernels for 0%

profile of v1, /device:TPU:0, one launch (start us, length us, event | category | flops | bytes accessed | tf_op | source)
XLA Modules:
  0.0 198.1 jit_solution(2129722699150659959)
XLA Ops:
  0.0 2.2 %fusion = f32[256]{0:T(256)S(1)} fusion(bf16[256,4096]{1,0:T(8,128)(2,1)} %param.12), kind=kLoop, calls=%fused_computation.2 | loop fusion | flops 3145472 | bytes 2098176 | tf_op jit(solution)/shard_map/reduce_sum | solution.py:983
  2.3 1.0 copy.53
  3.3 0.1 copy.52
  3.5 0.3 maximum_bitcast_fusion
  3.8 0.9 copy.54
  4.7 2.0 fusion.2.normed
  6.7 91.6 %shard_map.118 = (bf16[1024,4096]{1,0:T(8,128)(2,1)}, bf16[4096,512]{1,0:T(8,128)(2,1)}, bf16[2,256,1024]{2,1,0:T(8,128)(2,1)}, bf16[2048,512]{1,0:T(8,128)(2,1)}) custom-call(bf16[256,4096]{1,0:T(8,128)(2,1)} %fusion.2.normed, bf16[512,512]{1,0:T(8,128)(2,1)} %w_query.1, bf16[512,512]{1,0:T(8,128)(2,1)} %w_glu.1, bf16[512,512]{1,0:T(8,128)(2,1)} %w_gate.1, ...), custom_call_target="tpu_custom_call" | custom-call | tf_op jit(solution)/shard_map/pallas_call | solution.py:667
  98.2 8.3 %fusion.39 = f32[1024,512]{0,1:T(8,128)S(1)} fusion(bf16[1024,4096]{1,0:T(8,128)(2,1)} %get-tuple-element.8, bf16[4096,512]{1,0:T(8,128)(2,1)} %get-tuple-element.9), kind=kOutput, calls=%fused_computation.82 | convolution fusion | flops 4294967296 | bytes 14680064 | tf_op jit(solution)/shard_map/dot_general | solution.py:996
  106.6 0.2 fusion.34
  106.8 0.2 copy.57
  107.2 0.6 fusion.25
  107.8 0.2 copy.56
  108.0 0.2 copy.55
  108.2 0.2 reshape.300
  108.4 0.2 copy.58
  108.7 0.3 fusion.23
  109.0 0.6 collective-permute-start
  109.6 0.5 multiply_cosine_fusion
  110.1 0.1 slice.79
  110.2 0.1 add.133
  110.5 0.6 dynamic-slice
  111.8 0.2 dynamic-update-slice
  112.0 5.8 %all-reduce.1 = f32[32]{0:T(128)S(1)} all-reduce(f32[32]{0:T(128)S(1)} %dynamic-update-slice), channel_id=1, replica_groups=mesh['sp'=8,'tp'=4] {'tp'}, use_global_device_ids=true, to_apply=%add.1 | all-reduce | flops 32 | bytes 256
  117.8 0.1 fusion.28
  118.0 0.1 dynamic_slice.6
  118.1 0.7 fusion.6
  118.8 6.1 %all_gather.7 = f32[32,2048]{1,0:T(8,128)S(1)} all-gather(f32[32,512]{1,0:T(8,128)S(1)} %pad_maximum_fusion.5), channel_id=1, replica_groups=mesh['sp'=8,'tp'=4] {'tp'}, dimensions={1}, use_global_device_ids=true | all-gather | bytes 327680 | tf_op jit(solution)/shard_map/all_gather | solution.py:1056
  124.9 0.6 dynamic-slice.2.gain
  125.6 0.2 pad_select_fusion
  125.7 0.1 fusion.37
  125.9 0.1 copy.59
  126.1 0.2 fusion.36
  126.3 0.3 pad_maximum_fusion
  126.6 0.1 copy.64
  126.8 0.2 fusion.35
  127.0 0.3 pad_maximum_fusion.1
  127.3 0.5 fusion.38
  128.0 0.3 fusion.3
  128.3 0.1 exponential_add_fusion
  128.4 0.5 fusion.4
  128.9 0.4 copy.79
  129.3 0.9 reshape.317.att
  130.2 2.2 %fusion.33 = (f32[4,256]{0,1:T(8,128)S(1)}, f32[4,256]{0,1:T(8,128)S(1)}, f32[4,256,128]{2,0,1:T(4,128)S(1)}) fusion(f32[31,1,128]{2,0,1:T(8,128)S(1)} %dynamic-slice_bitcast_fusion, bf16[4,256,128]{2,0,1:T(4,128)(2,1)S(1)} %copy.58, bf16[4,30,128]{2,0,1:T(4,128)(2,1)S(1)} %slice-done), kind=kOutput, calls=%fused_computation.76 | convolution fusion | flops 49735680 | bytes 841216 | tf_op jit(solution)/shard_map/conv_general_dilated | solution.py:1058
  132.4 0.8 copy.72
  133.4 0.1 copy.73
  133.5 0.6 pad_maximum_fusion.6.stats
  134.1 62.1 %shard_map.119 = bf16[256,1024]{1,0:T(8,128)(2,1)} custom-call(bf16[1024,128]{1,0:T(8,128)(2,1)} %reshape.317.att, f32[1024,128]{1,0:T(8,128)} %bitcast.62, f32[16,128]{1,0:T(8,128)} %pad_maximum_fusion.6.stats, f32[1,128]{1,0:T(1,128)} %dynamic-slice.2.gain, bf16[256,1024]{1,0:T(8,128)(2,1)} %out_attn.3, bf16[256,1024]{1,0:T(8,128)(2,1)} %out_conv.3, ...), custom_call_target="tpu_custom_call" | custom-call | tf_op jit(solution)/shard_map/pallas_call | solution.py:935
  196.2 1.9 copy.95
  (54 shorter events, 1.1 us)
Async XLA Ops:
  0.0 4.7 %copy-start = (bf16[256,4096]{1,0:T(8,128)(2,1)S(1)}, bf16[256,4096]{1,0:T(8,128)(2,1)}, u32[]{:S(2)}) copy-start(bf16[256,4096]{1,0:T(8,128)(2,1)} %param.12) | copy-start | bytes 6291460
  0.0 3.3 %copy-start.2 = (bf16[512,128]{1,0:T(8,128)(2,1)S(1)}, bf16[512,128]{1,0:T(8,128)(2,1)}, u32[]{:S(2)}) copy-start(bf16[512,128]{1,0:T(8,128)(2,1)} %param.15) | copy-start | bytes 393220
  0.0 4.7 %copy-start.4 = (f32[4096]{0:T(1024)S(1)}, f32[4096]{0:T(1024)}, u32[]{:S(2)}) copy-start(f32[4096]{0:T(1024)} %param.13) | copy-start | bytes 49156
  107.1 3.4 %copy-start.7 = (u32[32]{0:T(128)S(1)}, u32[32]{0:T(128)}, u32[]{:S(2)}) copy-start(u32[32]{0:T(128)} %constant.84) | copy-start | bytes 388
  107.1 4.7 %copy-start.6 = (f32[8]{0:T(128)S(1)}, f32[8]{0:T(128)}, u32[]{:S(2)}) copy-start(f32[8]{0:T(128)} %param.19) | copy-start | bytes 100
  107.1 10.7 %copy-start.3 = (bf16[31,512]{1,0:T(8,128)(2,1)S(1)}, bf16[31,512]{1,0:T(8,128)(2,1)}, u32[]{:S(2)}) copy-start(bf16[31,512]{1,0:T(8,128)(2,1)} %param.20) | copy-start | bytes 95236
  108.4 9.7 %copy-start.5 = (f32[512]{0:T(512)S(1)}, f32[512]{0:T(512)}, u32[]{:S(2)}) copy-start(f32[512]{0:T(512)} %param.21) | copy-start | bytes 6148
  109.0 16.6 %collective-permute-start = (bf16[4,158,128]{2,0,1:T(4,128)(2,1)S(1)}, bf16[4,158,128]{2,0,1:T(4,128)(2,1)S(1)}, u32[]{:S(2)}, u32[]{:S(2)}) collective-permute-start(bf16[4,158,128]{2,0,1:T(4,128)(2,1)S(1)} %fusion.23), channel_id=1, source_target_pairs={{0,4},{4,0},{8,12},{12,8},{16,20},{20,16},{24,28},{28,24},{1,5},{5... | collective-permute-start | bytes 485384 | tf_op jit(solution)/shard_map/ppermute | solution.py:1017
  125.7 1.1 copy-start.1
  128.4 1.9 slice-start

commit v2 on v0

--- a/solution.py
+++ b/solution.py
@@ -147,7 +147,7 @@
     )(*arrays)
 
 
-def per_device(
+def gathered_per_device(
     tokens,
     norm_gain,
     w_query,
@@ -259,9 +259,852 @@
     return mixed.astype(jnp.bfloat16)
 
 
+MESH = pl.DeviceIdType.MESH
+A_CHUNKS = 2
+OUT_CHUNKS = 2
+LANES = 128
+
+
+def remote(src, dst, sems, index, target, send_index=None):
+    send_sem, recv_sem = sems
+    return pltpu.make_async_remote_copy(
+        src_ref=src,
+        dst_ref=dst,
+        send_sem=send_sem.at[index if send_index is None else send_index],
+        recv_sem=recv_sem.at[index],
+        device_id=target,
+        device_id_type=MESH,
+    )
+
+
+def layer_kernel(planes, channels, *refs):
+    (tokens, norm_gain, freq, w_key, w_value, taps, conv_gain, sink) = refs[:8]
+    (w_query, w_glu, w_gate, out_attn, out_conv) = refs[8:13]
+    mixed = refs[13]
+    (rows_all, w_all, stage, w_kv, small_src, small) = refs[14:20]
+    (acc, cosine, sine, q_b, kv_b, kv_rim, gated, gated_rim, extended, filtered) = refs[20:30]
+    (act, weights, stats, stats_all, moments, in_up, in_down, outgoing) = refs[30:38]
+    local_sem = refs[38]
+    pairs = [(refs[39 + 2 * i], refs[40 + 2 * i]) for i in range((len(refs) - 39) // 2)]
+    (a_sem, ax_sem, ac_sem, w1_sem, w2_sem, w3_sem, kc_sem, o_sem, small_sem) = pairs[:9]
+    (halo_sem, s_sem, x_sem, c_sem, r_sem) = pairs[9:14]
+
+    s, t = lax.axis_index("sp"), lax.axis_index("tp")
+    z, y, x, c = s // 2, s % 2, t // 2, t % 2
+    block = tokens.shape[0]
+    rows = planes * block
+    piece = block // planes
+    step = piece // A_CHUNKS
+    depth = w_query.shape[0]
+    width = w_query.shape[1] // planes
+    three = 3 * width
+    half = depth // 2
+    heads = width // HEAD
+    group = out_attn.shape[0]
+    part = planes * width
+    size = planes * planes
+    f32 = jnp.float32
+
+    def at(zz, yy, tt):
+        return {"sp": zz * 2 + yy, "tp": tt}
+
+    tx, td, tp = (1 - x) * 2 + c, (1 - x) * 2 + (1 - c), x * 2 + (1 - c)
+    across_y, across_x = at(z, 1 - y, t), at(z, y, tx)
+    diagonal, partner = at(z, y, td), at(z, y, tp)
+    mine = z * planes + t
+    peers = [lax.rem(mine + k, size) for k in range(1, size)]
+
+    barrier = pltpu.get_barrier_semaphore()
+    for target in [across_y] + [at(g // planes, y, g % planes) for g in peers]:
+        pl.semaphore_signal(barrier, inc=1, device_id=target, device_id_type=MESH)
+
+    def normalise(start, count):
+        @pl.loop(0, count // 16)
+        def _(i):
+            here = pl.multiple_of(start + i * 16, 16)
+            value = tokens[pl.ds(here, 16), :].astype(f32)
+            scale = lax.rsqrt(jnp.mean(value * value, axis=1, keepdims=True) + 1e-06)
+            there = pl.multiple_of(z * block + here, 16)
+            rows_all[pl.ds(there, 16), :] = (value * scale * norm_gain[...]).astype(rows_all.dtype)
+
+    normalise(t * piece, piece)
+
+    lane = lax.broadcasted_iota(jnp.int32, (half, 2 * HEAD), 1)
+    for cc in range(2):
+        key = w_key[cc * half : (cc + 1) * half, :].astype(f32)
+        value = w_value[cc * half : (cc + 1) * half, :].astype(f32)
+        w_kv[cc] = jnp.where(lane < HEAD, key, pltpu.roll(value, HEAD, 1)).astype(w_kv.dtype)
+        w_kv[2 + cc] = jnp.where(lane < HEAD, pltpu.roll(key, HEAD, 1), value).astype(w_kv.dtype)
+    small_src[...] = jnp.zeros_like(small_src)
+    for tt in range(planes):
+        cols = slice(tt * width, (tt + 1) * width)
+        small_src[tt, 0:KSIZE, :] = taps[:, cols].astype(f32)
+        small_src[tt, 32:33, :] = conv_gain[:, cols]
+        small_src[tt, 33:34, 0 : sink.shape[1]] = sink[...]
+    pl.semaphore_wait(barrier, size)
+
+    def rows_of(zz, tt, chunk):
+        start = pl.multiple_of(zz * block + tt * piece + chunk * step, step)
+        return rows_all.at[pl.ds(start, step)]
+
+    def origin(way, distance):
+        return z - distance if way == 0 else z + distance
+
+    def chain(way, distance, chunk):
+        ref = rows_of(origin(way, distance), t, chunk)
+        index = (way * planes + distance) * A_CHUNKS + chunk
+        return remote(ref, ref, a_sem, index, at(z + 1 if way == 0 else z - 1, y, t))
+
+    def chain_arrival(way, distance, chunk):
+        ref = rows_of(origin(way, distance), t, chunk)
+        index = (way * planes + distance - 1) * A_CHUNKS + chunk
+        return remote(ref, ref, a_sem, index, across_x)
+
+    def can_send(way, distance):
+        if way == 0:
+            return jnp.logical_and(z - distance >= 0, z + 1 < planes)
+        return jnp.logical_and(z + distance < planes, z - 1 >= 0)
+
+    def exists(way, distance):
+        return z - distance >= 0 if way == 0 else z + distance < planes
+
+    def sideways(way, distance, chunk, arrival=False):
+        ref = rows_of(origin(way, distance), tx if arrival else t, chunk)
+        index = (way * planes + distance) * A_CHUNKS + chunk
+        return remote(ref, ref, ax_sem, index, across_x)
+
+    def to_partner(way, distance, chunk, far, arrival=False):
+        tt = (td if far else tp) if arrival else (tx if far else t)
+        ref = rows_of(origin(way, distance), tt, chunk)
+        index = ((way * planes + distance) * A_CHUNKS + chunk) * 2 + far
+        return remote(ref, ref, ac_sem, index, partner)
+
+    def home(zz, yy):
+        return pl.multiple_of((zz * 2 + yy) * depth, depth)
+
+    def wide(ref, start):
+        return ref.at[pl.ds(start, depth), pl.ds(0, three)]
+
+    def narrow(ref, start, cc):
+        return ref.at[pl.ds(pl.multiple_of(start + cc * half, half), half), pl.ds(three, width)]
+
+    def w_sources(tt):
+        cols = pl.ds(pl.multiple_of(tt * width, width), width)
+        return [w_query.at[:, cols], w_glu.at[:, cols], w_gate.at[:, cols], w_kv.at[tt]]
+
+    def w_targets(ref, start, cc):
+        here = pl.ds(start, depth)
+        return [ref.at[here, pl.ds(g * width, width)] for g in range(3)] + [narrow(ref, start, cc)]
+
+    def first_all(kind, target, tt, what):
+        for here, ref, start in (
+            (t == z, w_all, home(z, y)),
+            (t != z, stage, pl.multiple_of(t * depth, depth)),
+        ):
+            @pl.when(here)
+            def _():
+                for i, (a, b) in enumerate(zip(w_sources(tt), w_targets(ref, start, tt % 2))):
+                    what(remote(a, b, w1_sem, kind * 4 + i, target))
+
+    def first_arrival(kind, src_t):
+        for here, ref, start in (
+            (src_t == z, w_all, home(z, y)),
+            (src_t != z, stage, pl.multiple_of(src_t * depth, depth)),
+        ):
+            @pl.when(here)
+            def _():
+                for i, b in enumerate(w_targets(ref, start, c)):
+                    remote(b, b, w1_sem, kind * 4 + i, across_x).wait_recv()
+
+    def second_local():
+        return [
+            remote(a, b, w2_sem, z * 4 + i, at(t, y, t), t * 4 + i)
+            for i, (a, b) in enumerate(zip(w_sources(t), w_targets(w_all, home(z, y), c)))
+        ]
+
+    def second_staged(src_t):
+        start = pl.multiple_of(src_t * depth, depth)
+        return [
+            remote(a, b, w2_sem, z * 4 + i, at(src_t, y, t), src_t * 4 + i)
+            for a, b, i in (
+                (wide(stage, start), wide(w_all, home(z, y)), 0),
+                (narrow(stage, start, c), narrow(w_all, home(z, y), c), 3),
+            )
+        ]
+
+    def second_arrival(from_z):
+        start = home(from_z, y)
+
+        @pl.when(t == z)
+        def _():
+            for i, ref in enumerate(w_targets(w_all, start, c)):
+                remote(ref, ref, w2_sem, from_z * 4 + i, across_x).wait_recv()
+
+        @pl.when(t != z)
+        def _():
+            for ref, i in ((wide(w_all, start), 0), (narrow(w_all, start, c), 3)):
+                remote(ref, ref, w2_sem, from_z * 4 + i, across_x).wait_recv()
+
+    def third(from_z, arrival=False):
+        start = home(from_z, 1 - y if arrival else y)
+        return [
+            remote(ref, ref, w3_sem, from_z * 2 + i, across_y)
+            for i, ref in enumerate((narrow(w_all, start, c), wide(w_all, start)))
+        ]
+
+    def to_share(from_z, own, arrival=False):
+        ref = narrow(w_all, home(from_z, y if own else 1 - y), 1 - c if arrival else c)
+        return remote(ref, ref, kc_sem, from_z * 2 + own, partner)
+
+    def out_copies(yy):
+        low = pl.multiple_of(yy * group, group)
+        high = pl.multiple_of(part + yy * group, group)
+        return [weights.at[pl.ds(low, group)], weights.at[pl.ds(high, group)]]
+
+    outs = [
+        remote(a, b, o_sem, i, across_y)
+        for i, (a, b) in enumerate(zip((out_attn, out_conv), out_copies(y)))
+    ]
+    out_loads = [
+        pltpu.make_async_copy(a, b, local_sem.at[4 + i])
+        for i, (a, b) in enumerate(zip((out_attn, out_conv), out_copies(y)))
+    ]
+    own_loads = [
+        pltpu.make_async_copy(a, b, local_sem.at[i])
+        for i, (a, b) in enumerate(zip(w_sources(t)[:3], w_targets(w_all, home(z, y), c)))
+    ]
+
+    for chunk in range(A_CHUNKS):
+        for way in range(2):
+            @pl.when(can_send(way, 0))
+            def _():
+                chain(way, 0, chunk).start()
+    small_to = [(partner, tp, 0), (across_x, tx, 1), (diagonal, td, 2)]
+
+    def small_copy(target, tt, i):
+        return pltpu.make_async_remote_copy(
+            src_ref=small_src.at[tt],
+            dst_ref=small,
+            send_sem=small_sem[0].at[i],
+            recv_sem=small_sem[1].at[0],
+            device_id=target,
+            device_id_type=MESH,
+        )
+
+    @pl.when(t == z)
+    def _():
+        for args in small_to:
+            small_copy(*args).start()
+        small[...] = small_src[t]
+
+    first_all(2, partner, tp, lambda copy: copy.start())
+    first_all(0, across_x, tx, lambda copy: copy.start())
+    first_all(1, diagonal, td, lambda copy: copy.start())
+    for copy in outs:
+        copy.start()
+    for copy in out_loads:
+        copy.start()
+
+    @pl.when(t == z)
+    def _():
+        for copy in own_loads:
+            copy.start()
+        start = pl.multiple_of(home(z, y) + c * half, half)
+        w_all[pl.ds(start, half), three : three + width] = w_kv[t]
+        for copy in own_loads:
+            copy.wait()
+
+    def toward(target, way):
+        return target > z if way == 0 else target < z
+
+    def send_second(way):
+        @pl.when(toward(t, way))
+        def _():
+            for copy in second_local():
+                copy.start()
+
+        for src_t in (tp, tx, td):
+            @pl.when(toward(src_t, way))
+            def _():
+                for copy in second_staged(src_t):
+                    copy.start()
+
+    def first_arrivals():
+        first_arrival(2, tp)
+        first_arrival(0, tx)
+        first_arrival(1, td)
+
+    def chain_step(distance):
+        for chunk in range(A_CHUNKS):
+            for way in range(2):
+                @pl.when(exists(way, distance))
+                def _():
+                    chain_arrival(way, distance, chunk).wait_recv()
+
+                    @pl.when(can_send(way, distance))
+                    def _():
+                        chain(way, distance, chunk).start()
+
+                    sideways(way, distance, chunk).start()
+                    to_partner(way, distance, chunk, 0).start()
+
+    def sideways_step(distance):
+        for chunk in range(A_CHUNKS):
+            for way in range(2):
+                @pl.when(exists(way, distance))
+                def _():
+                    sideways(way, distance, chunk, True).wait_recv()
+                    to_partner(way, distance, chunk, 1).start()
+
+    def settle(from_z):
+        to_share(from_z, 1).start()
+        for copy in third(from_z):
+            copy.start()
+
+    def plane_step(distance):
+        for way in range(2):
+            @pl.when(exists(way, distance))
+            def _():
+                second_arrival(origin(way, distance))
+                settle(origin(way, distance))
+
+    ends = jnp.logical_or(z == 0, z == planes - 1)
+
+    @pl.when(ends)
+    def _():
+        first_arrivals()
+        for way in range(2):
+            send_second(way)
+
+    for k in range(1, planes):
+        normalise(lax.rem(t + k, planes) * piece, piece)
+    for distance in range(1, planes - 1):
+        chain_step(distance)
+        if distance == 1:
+            @pl.when(jnp.logical_not(ends))
+            def _():
+                first_arrivals()
+
+            settle(z)
+        for way in range(2):
+            @pl.when(jnp.logical_and(jnp.logical_not(ends), z == (distance if way == 0 else planes - 1 - distance)))
+            def _():
+                send_second(way)
+
+    row = lax.broadcasted_iota(jnp.int32, (block, LANES), 0)
+    for zz in range(planes):
+        angle = ((2 * zz + y) * block + row).astype(f32) * freq[...]
+        here = slice(zz * block, (zz + 1) * block)
+        cosine[here, :] = jnp.cos(angle)
+        sine[here, :] = jnp.sin(angle)
+
+    chain_step(planes - 1)
+    plane_step(1)
+    sideways_step(1)
+    plane_step(2)
+    for distance in range(2, planes):
+        sideways_step(distance)
+    for distance in range(3, planes):
+        plane_step(distance)
+    for distance in range(1, planes):
+        for chunk in range(A_CHUNKS):
+            for way in range(2):
+                @pl.when(exists(way, distance))
+                def _():
+                    for far in range(2):
+                        to_partner(way, distance, chunk, far, True).wait_recv()
+
+    ahead = 1 - 2 * (z // (planes // 2))
+    tall = rows // 2
+
+    def multiply(from_z, yy, fresh):
+        start = home(from_z, yy)
+        cols = pl.ds(start, depth)
+
+        @pl.loop(0, 2)
+        def _(i):
+            here = pl.ds(pl.multiple_of(i * tall, tall), tall)
+            value = jnp.dot(rows_all[here, cols], w_all[cols, :], preferred_element_type=f32)
+            if fresh:
+                acc[here, :] = value
+            else:
+                acc[here, :] += value
+
+    to_share(z, 1, True).wait_recv()
+    multiply(z, y, True)
+
+    @pl.loop(1, planes)
+    def _(k):
+        from_z = lax.rem(z + k * ahead + planes, planes)
+        to_share(from_z, 1, True).wait_recv()
+        multiply(from_z, y, False)
+
+    @pl.loop(0, planes)
+    def _(k):
+        from_z = lax.rem(z + k * ahead + planes, planes)
+        narrow_copy, wide_copy = third(from_z, True)
+        narrow_copy.wait_recv()
+        to_share(from_z, 0).start()
+        wide_copy.wait_recv()
+        to_share(from_z, 0, True).wait_recv()
+        multiply(from_z, 1 - y, False)
+
+    lane = lax.broadcasted_iota(jnp.int32, (block, LANES), 1)
+    low = lax.rem(lane, HEAD) < HEAD // 2
+
+    def turned(value, here):
+        other = jnp.where(low, -pltpu.roll(value, LANES - HEAD // 2, 1), pltpu.roll(value, HEAD // 2, 1))
+        return value * cosine[here, :] + other * sine[here, :]
+
+    def halo(kind, zz):
+        if kind == 0:
+            ref = kv_b.at[pl.ds((zz + 1) * block - WINDOW, WINDOW)]
+            return remote(ref, kv_rim.at[zz + y], halo_sem, zz, across_y)
+        ref = gated.at[pl.ds((zz + 1) * block - 32, 32)]
+        return remote(ref, gated_rim.at[zz + y], halo_sem, planes + zz, across_y)
+
+    def halo_arrival(kind, zz):
+        ref = (kv_rim if kind == 0 else gated_rim).at[zz + 1 - y]
+        return remote(ref, ref, halo_sem, kind * planes + zz, across_y)
+
+    for zz in range(planes):
+        here = slice(zz * block, (zz + 1) * block)
+        value = acc[here, three:]
+        kv_b[here, :] = jnp.where(lane < HEAD, turned(value, here), value).astype(kv_b.dtype)
+        halo(0, zz).start()
+    for zz in range(planes):
+        here = slice(zz * block, (zz + 1) * block)
+        gate = acc[here, 2 * width : three]
+        value = (acc[here, width : 2 * width] * (1.0 / (1.0 + jnp.exp(-gate)))).astype(gated.dtype)
+        gated[here, :] = value
+        extended[zz, 32:, :] = value.astype(f32)
+        halo(1, zz).start()
+
+    @pl.when(y == 0)
+    def _():
+        kv_rim[0] = jnp.zeros_like(kv_rim[0])
+        gated_rim[0] = jnp.zeros_like(gated_rim[0])
+
+    for zz in range(planes):
+        here = slice(zz * block, (zz + 1) * block)
+        q_b[here, :] = (turned(acc[here, :width], here) * (1.0 / math.sqrt(HEAD))).astype(q_b.dtype)
+
+    @pl.when(t != z)
+    def _():
+        small_copy(partner, tp, 0).wait_recv()
+
+    lane_q = lax.broadcasted_iota(jnp.int32, (WINDOW, LANES), 1)
+    lane_k = lax.broadcasted_iota(jnp.int32, (2 * WINDOW, LANES), 1)
+    row_s = lax.rem(lax.broadcasted_iota(jnp.int32, (heads * WINDOW, 2 * WINDOW), 0), WINDOW)
+    col_s = lax.broadcasted_iota(jnp.int32, (heads * WINDOW, 2 * WINDOW), 1)
+    distance_s = row_s + WINDOW - col_s
+    inside = jnp.logical_and(distance_s >= 0, distance_s < WINDOW)
+    sink_row = small[33:34, :]
+    lane_1 = lax.broadcasted_iota(jnp.int32, (1, LANES), 1)
+    sinks = [
+        jnp.sum(jnp.where(lane_1 == t * heads + h, sink_row, 0.0), axis=1, keepdims=True)
+        for h in range(heads)
+    ]
+    sink_col = jnp.concatenate([jnp.broadcast_to(v, (WINDOW, 1)) for v in sinks], axis=0)
+
+    def attend(first_row, keys, mask):
+        query = q_b[pl.ds(first_row, WINDOW), :]
+        keys_f = keys.astype(f32)
+        swapped = pltpu.roll(keys_f, HEAD, 1)
+        key_two = jnp.where(lane_k < HEAD, keys_f, swapped).astype(jnp.bfloat16)
+        value_two = jnp.where(lane_k < HEAD, swapped, keys_f).astype(jnp.bfloat16)
+        zero = jnp.zeros_like(query)
+        stacked = jnp.concatenate(
+            [jnp.where(lane_q // HEAD == h, query, zero) for h in range(heads)], axis=0
+        )
+        scores = lax.dot_general(
+            stacked, key_two, (((1,), (1,)), ((), ())), preferred_element_type=f32
+        )
+        scores = jnp.where(mask, scores, -1e30)
+        top = jnp.maximum(jnp.max(scores, axis=1, keepdims=True), sink_col)
+        grown = jnp.exp(scores - top)
+        total = jnp.sum(grown, axis=1, keepdims=True) + jnp.exp(sink_col - top)
+        probs = (grown / total).astype(jnp.bfloat16)
+        mixed_values = jnp.dot(probs, value_two, preferred_element_type=f32)
+        result = mixed_values[:WINDOW]
+        for h in range(1, heads):
+            result = jnp.where(lane_q // HEAD == h, mixed_values[h * WINDOW : (h + 1) * WINDOW], result)
+        act[pl.ds(first_row, WINDOW), columns(0, t)] = result.astype(act.dtype)
+
+    def columns(kind, tt):
+        return pl.ds(pl.multiple_of(kind * part + tt * width, width), width)
+
+    blocks = block // WINDOW
+
+    @pl.loop(0, planes)
+    def _(zz):
+        for b in range(1, blocks):
+            start = pl.multiple_of(zz * block + b * WINDOW, WINDOW)
+            before = pl.multiple_of(zz * block + (b - 1) * WINDOW, WINDOW)
+            attend(start, kv_b[pl.ds(before, 2 * WINDOW), :], inside)
+
+    for zz in range(planes):
+        if zz < planes - 1:
+            halo_arrival(1, zz).wait_recv()
+
+        @pl.when(y == 1)
+        def _():
+            if zz == planes - 1:
+                halo_arrival(1, zz).wait_recv()
+
+    for zz in range(planes):
+        extended[zz, 0:32, :] = gated_rim[zz].astype(f32)
+    strip = 64
+
+    @pl.loop(0, planes)
+    def _(zz):
+        @pl.loop(0, block // strip)
+        def _(i):
+            base = pl.multiple_of(i * strip, strip)
+            window = extended[zz, pl.ds(base, strip + 32), :]
+            total = window[2 : 2 + strip] * small[0:1, :]
+            for k in range(1, KSIZE):
+                total = total + window[2 + k : 2 + k + strip] * small[k : k + 1, :]
+            filtered[pl.ds(pl.multiple_of(zz * block + base, strip), strip), :] = total
+
+    tiles = rows // LANES
+    for k in range(tiles):
+        value = filtered[k * LANES : (k + 1) * LANES, :]
+        total = jnp.sum(value, axis=1, keepdims=True)
+        square = jnp.sum(value * value, axis=1, keepdims=True)
+        stats[k : k + 1, :] = jnp.transpose(jnp.broadcast_to(total, (LANES, LANES)))[0:1]
+        stats[tiles + k : tiles + k + 1, :] = jnp.transpose(jnp.broadcast_to(square, (LANES, LANES)))[0:1]
+
+    def stat(k):
+        g = peers[k]
+        return pltpu.make_async_remote_copy(
+            src_ref=stats,
+            dst_ref=stats_all.at[mine],
+            send_sem=s_sem[0].at[k],
+            recv_sem=s_sem[1].at[mine],
+            device_id=at(g // planes, y, g % planes),
+            device_id_type=MESH,
+        )
+
+    for k in range(size - 1):
+        stat(k).start()
+    stats_all[mine] = stats[...]
+
+    for zz in range(planes):
+        if zz < planes - 1:
+            halo_arrival(0, zz).wait_recv()
+
+        @pl.when(y == 1)
+        def _():
+            if zz == planes - 1:
+                halo_arrival(0, zz).wait_recv()
+
+    @pl.loop(0, planes)
+    def _(zz):
+        start = pl.multiple_of(zz * block, block)
+        keys = jnp.concatenate([kv_rim[zz], kv_b[pl.ds(start, WINDOW), :]], axis=0)
+        began = jnp.logical_or(zz * 2 + y > 0, col_s >= WINDOW)
+        attend(start, keys, jnp.logical_and(inside, began))
+
+    def region(kind, r, tt):
+        start = pl.multiple_of(r * block, block)
+        return act.at[pl.ds(start, block), columns(kind, tt)]
+
+    def cross(kind, r, arrival=False):
+        ref = region(kind, r, tx if arrival else t)
+        return remote(ref, ref, x_sem, kind * planes + r, across_x)
+
+    def hand(kind, r, far, arrival=False):
+        tt = (td if far else tp) if arrival else (tx if far else t)
+        ref = region(kind, r, tt)
+        return remote(ref, ref, c_sem, (kind * planes + r) * 2 + far, partner)
+
+    near = z // (planes // 2)
+    order = [(1 - near) * (planes - 1 - j) + near * j for j in range(planes)]
+    for r in order:
+        cross(0, r).start()
+        hand(0, r, 0).start()
+    for g in peers:
+        ref = stats_all.at[g]
+        pltpu.make_async_remote_copy(
+            src_ref=ref,
+            dst_ref=ref,
+            send_sem=s_sem[0].at[0],
+            recv_sem=s_sem[1].at[g],
+            device_id=partner,
+            device_id_type=MESH,
+        ).wait_recv()
+    total = stats_all[0]
+    for g in range(1, size):
+        total = total + stats_all[g]
+    mean = total[:tiles] / channels
+    variance = total[tiles:] / channels - mean * mean
+    moments[0] = mean
+    moments[1] = lax.rsqrt(variance + 1e-05)
+    per = block // LANES
+
+    def normed_out(r):
+        for k in range(per):
+            tile = r * per + k
+            mean_col = jnp.transpose(jnp.broadcast_to(moments[0, pl.ds(tile, 1), :], (LANES, LANES)))
+            rate_col = jnp.transpose(jnp.broadcast_to(moments[1, pl.ds(tile, 1), :], (LANES, LANES)))
+            here = pl.ds(pl.multiple_of(tile * LANES, LANES), LANES)
+            scaled = (filtered[here, :] - mean_col) * rate_col * small[32:33, :]
+            act[here, columns(1, t)] = (scaled / (1.0 + jnp.exp(-scaled))).astype(act.dtype)
+
+    for r in order:
+        normed_out(r)
+        cross(1, r).start()
+        hand(1, r, 0).start()
+    for copy in out_loads:
+        copy.wait()
+    for copy in outs:
+        copy.wait_recv()
+    for kind in range(2):
+        for r in order:
+            cross(kind, r, True).wait_recv()
+            hand(kind, r, 1).start()
+    for kind in range(2):
+        for r in order:
+            for far in range(2):
+                hand(kind, r, far, True).wait_recv()
+
+    out_step = block // OUT_CHUNKS
+    columns_out = mixed.shape[1]
+    tile_out = min(256, columns_out)
+
+    def partial(r, h, tile):
+        start = pl.multiple_of(r * block + h * out_step, out_step)
+        cols = pl.ds(pl.multiple_of(tile * tile_out, tile_out), tile_out)
+        value = jnp.dot(act[pl.ds(start, out_step), :], weights[:, cols], preferred_element_type=f32)
+        return value, cols
+
+    def travel(way, r, h, arrival=False):
+        rows_h = pl.ds(h * out_step, out_step)
+        into = (in_up if way == 0 else in_down).at[r, rows_h]
+        index = (way * planes + r) * OUT_CHUNKS + h
+        source = into if arrival else outgoing.at[r, rows_h]
+        return remote(source, into, r_sem, index, across_y if arrival else at(z + 1 if way == 0 else z - 1, y, t))
+
+    for distance in range(planes - 1, 0, -1):
+        for h in range(OUT_CHUNKS):
+            rows_h = pl.ds(h * out_step, out_step)
+            for way in range(2):
+                r = z + distance if way == 0 else z - distance
+                there = r < planes if way == 0 else r >= 0
+                more = z > 0 if way == 0 else z < planes - 1
+                into = in_up if way == 0 else in_down
+
+                @pl.when(jnp.logical_and(there, jnp.logical_not(more)))
+                def _():
+                    @pl.loop(0, columns_out // tile_out)
+                    def _(tile):
+                        value, cols = partial(r, h, tile)
+                        outgoing[r, rows_h, cols] = value.astype(outgoing.dtype)
+
+                    travel(way, r, h).start()
+
+                @pl.when(jnp.logical_and(there, more))
+                def _():
+                    travel(way, r, h, True).wait_recv()
+
+                    @pl.loop(0, columns_out // tile_out)
+                    def _(tile):
+                        value, cols = partial(r, h, tile)
+                        outgoing[r, rows_h, cols] = (value + into[r, rows_h, cols].astype(f32)).astype(
+                            outgoing.dtype
+                        )
+
+                    travel(way, r, h).start()
+
+    for h in range(OUT_CHUNKS):
+        rows_h = pl.ds(h * out_step, out_step)
+
+        @pl.when(z > 0)
+        def _():
+            travel(0, z, h, True).wait_recv()
+
+        @pl.when(z < planes - 1)
+        def _():
+            travel(1, z, h, True).wait_recv()
+
+        @pl.loop(0, columns_out // tile_out)
+        def _(tile):
+            value, cols = partial(z, h, tile)
+            below = in_up[z, rows_h, cols].astype(f32)
+            above = in_down[z, rows_h, cols].astype(f32)
+            value = value + jnp.where(z > 0, below, 0.0) + jnp.where(z < planes - 1, above, 0.0)
+            mixed[rows_h, cols] = value.astype(mixed.dtype)
+
+    @pl.when(t == z)
+    def _():
+        for args in small_to:
+            small_copy(*args).wait_send()
+
+    @pl.when(y == 0)
+    def _():
+        for kind in range(2):
+            halo(kind, planes - 1).wait_send()
+
+    @pl.when(y == 1)
+    def _():
+        for kind in range(2):
+            halo(kind, planes - 1).wait_send()
+
+    for zz in range(planes - 1):
+        for kind in range(2):
+            halo(kind, zz).wait_send()
+
+    @pl.when(y == 0)
+    def _():
+        for kind in range(2):
+            halo_arrival(kind, planes - 1).wait_recv()
+
+    for copy in outs:
+        copy.wait_send()
+    first_all(2, partner, tp, lambda copy: copy.wait_send())
+    first_all(0, across_x, tx, lambda copy: copy.wait_send())
+    first_all(1, diagonal, td, lambda copy: copy.wait_send())
+
+    @pl.when(t != z)
+    def _():
+        for copy in second_local():
+            copy.wait_send()
+
+    for src_t in (tp, tx, td):
+        @pl.when(src_t != z)
+        def _():
+            for copy in second_staged(src_t):
+                copy.wait_send()
+
+    for zz in range(planes):
+        for copy in third(zz):
+            copy.wait_send()
+        for own in range(2):
+            to_share(zz, own).wait_send()
+    for distance in range(planes):
+        for chunk in range(A_CHUNKS):
+            for way in range(2):
+                @pl.when(can_send(way, distance))
+                def _():
+                    chain(way, distance, chunk).wait_send()
+
+                if distance:
+                    @pl.when(exists(way, distance))
+                    def _():
+                        sideways(way, distance, chunk).wait_send()
+                        for far in range(2):
+                            to_partner(way, distance, chunk, far).wait_send()
+    for k in range(size - 1):
+        stat(k).wait_send()
+    for kind in range(2):
+        for r in order:
+            cross(kind, r).wait_send()
+            for far in range(2):
+                hand(kind, r, far).wait_send()
+    for distance in range(1, planes):
+        for h in range(OUT_CHUNKS):
+            for way in range(2):
+                r = z + distance if way == 0 else z - distance
+
+                @pl.when(r < planes if way == 0 else r >= 0)
+                def _():
+                    travel(way, r, h).wait_send()
+
+
+def planned_per_device(
+    tokens,
+    norm_gain,
+    w_query,
+    w_key,
+    w_value,
+    w_glu,
+    w_gate,
+    sink_logit,
+    conv_taps,
+    conv_gain,
+    out_attn,
+    out_conv,
+):
+    planes = lax.axis_size("tp")
+    block, model = tokens.shape
+    rows = planes * block
+    depth, cols = w_query.shape
+    width = cols // planes
+    columns_out = out_attn.shape[1]
+    size = planes * planes
+    half_width = HEAD // 2
+    freq = 10000.0 ** (-jnp.arange(half_width, dtype=jnp.float32) * 2.0 / HEAD)
+    freq = jnp.tile(freq, LANES // half_width)[None]
+    vmem = pl.BlockSpec(memory_space=pltpu.VMEM)
+    any_spec = pl.BlockSpec(memory_space=pl.ANY)
+    dma = pltpu.SemaphoreType.DMA
+    bf16, f32 = jnp.bfloat16, jnp.float32
+    tiles = rows // LANES
+    chunks = 2 * planes * A_CHUNKS
+    counts = [
+        chunks, chunks, 2 * chunks, 12, 4 * planes, 2 * planes, 2 * planes, 2, 3,
+        2 * planes, size, 2 * planes, 4 * planes, 2 * planes * OUT_CHUNKS,
+    ]
+    sems = [dma((n,)) for n in counts for _ in range(2)]
+    return pl.pallas_call(
+        functools.partial(layer_kernel, planes, CONV),
+        out_shape=jax.ShapeDtypeStruct((block, columns_out), bf16),
+        in_specs=[vmem] * 8 + [any_spec] * 5,
+        out_specs=vmem,
+        scratch_shapes=[
+            pltpu.VMEM((rows, model), bf16),
+            pltpu.VMEM((2 * planes * depth, 4 * width), bf16),
+            pltpu.VMEM((planes * depth, 4 * width), bf16),
+            pltpu.VMEM((planes, depth // 2, 2 * HEAD), bf16),
+            pltpu.VMEM((planes, 40, width), f32),
+            pltpu.VMEM((40, width), f32),
+            pltpu.VMEM((rows, 4 * width), f32),
+            pltpu.VMEM((rows, LANES), f32),
+            pltpu.VMEM((rows, LANES), f32),
+            pltpu.VMEM((rows, width), bf16),
+            pltpu.VMEM((rows, width), bf16),
+            pltpu.VMEM((planes + 1, WINDOW, width), bf16),
+            pltpu.VMEM((rows, width), bf16),
+            pltpu.VMEM((planes + 1, 32, width), bf16),
+            pltpu.VMEM((planes, 32 + block, width), f32),
+            pltpu.VMEM((rows, width), f32),
+            pltpu.VMEM((rows, 2 * planes * width), bf16),
+            pltpu.VMEM((2 * planes * width, columns_out), bf16),
+            pltpu.VMEM((2 * tiles, LANES), f32),
+            pltpu.VMEM((size, 2 * tiles, LANES), f32),
+            pltpu.VMEM((2, tiles, LANES), f32),
+            pltpu.VMEM((planes, block, columns_out), bf16),
+            pltpu.VMEM((planes, block, columns_out), bf16),
+            pltpu.VMEM((planes, block, columns_out), bf16),
+            dma((8,)),
+        ]
+        + sems,
+        compiler_params=pltpu.CompilerParams(
+            collective_id=0, has_side_effects=True, vmem_limit_bytes=60 * 2**20
+        ),
+    )(
+        tokens,
+        norm_gain[None],
+        freq,
+        w_key,
+        w_value,
+        conv_taps,
+        conv_gain[None],
+        sink_logit[None],
+        w_query,
+        w_glu,
+        w_gate,
+        out_attn,
+        out_conv,
+    )
+
+
 def solution(mesh):
+    planes, others = mesh.shape["tp"], mesh.shape["sp"]
+    fits = others == 2 * planes and planes % 2 == 0 and HEADS == 2 * planes * planes
     return jax.shard_map(
-        per_device,
+        planned_per_device if fits else gathered_per_device,
         mesh=mesh,
         in_specs=(
             P("sp", None),

time: 299 us -> 175 us (0.59)
  Pallas kernels: 224 us -> 171 us
  matrix products: 25.7 us -> 0 us
  waiting for transfers between devices: 15.6 us -> 0 us
  between operations: 13.8 us -> 0.01 us
  starting transfers between devices: 7.09 us -> 0 us
  blocking collectives: 5.67 us -> 0 us
  other arithmetic: 4.76 us -> 0.01 us
    pallas_call x1, Pallas kernels: 224 us -> 171 us  [planned_per_device(): pl.pallas_call(functools.partial(layer_kernel, planes, CONV), out_shape=j...]
    dot_general x9 -> x0, matrix products: 24.3 us -> none  [the longest x5 15 us: per_device(): jnp.dot(normed, weight_piece, preferred_element_type=jnp.float32)]
    all_gather x2 -> x0, waiting for transfers between devices: 14.2 us -> none  [the longest x1 14.1 us: per_device(): lax.all_gather(conv_out, 'tp', axis=1, tiled=True)]
    ppermute x2 -> x0, starting transfers between devices: 7.05 us -> none  [passed_along(): return lax.ppermute(block, axis, route)]
    psum x1 -> x0, blocking collectives: 5.67 us -> none  [per_device(): lax.psum((jnp.sum(filtered, axis=1), jnp.sum(filtered * filtered, axis=1)...]
  transfers between devices with their start and end apart: 4 -> 0, of which waited for: 2 -> 0; matrix products, arithmetic and copies ran while one was open for 7% -> 0% of each run, Pallas kernels for 0% -> 0%
where the time goes in v2:
time: 175 us; the launch traced here: 173 us
  Pallas kernels  171 us (98%)
  local copies, waits for them, and re-layouts  2.47 us (1%)
    pallas_call x1, Pallas kernels, planned_per_device(): pl.pallas_call(functools.partial(layer_kernel, planes, CONV), out_shape=j...  171 us

profile of v2, /device:TPU:0, one launch (start us, length us, event | category | flops | bytes accessed | tf_op | source)
XLA Modules:
  0.0 173.1 jit_solution(3261718843212739522)
XLA Ops:
  0.0 0.6 broadcast_in_dim_tile.3.refs_2_
  0.6 170.6 %shard_map.118 = bf16[256,1024]{1,0:T(8,128)(2,1)} custom-call(bf16[256,4096]{1,0:T(8,128)(2,1)} %refs_0_.1, f32[1,4096]{1,0:T(1,128)} %bitcast.3, f32[1,128]{1,0:T(1,128)} %broadcast_in_dim_tile.3.refs_2_, bf16[512,128]{1,0:T(8,128)(2,1)} %refs_3_.1, bf16[512,128]{1,0:T(8,128)(2,1)} %refs_4_.1, bf16[31,512]{1,0:T(8,128)(2,1)} %refs_5_.1, f32[1,512]{1,0:T(1,128)} %bitcast.4, ...), custom_call_target="tpu_custom_call" | custom-call | tf_op jit(solution)/shard_map/pallas_call | solution.py:1050
  171.2 1.9 %copy.14 = bf16[256,1024]{1,0:T(8,128)(2,1)} copy(bf16[256,1024]{1,0:T(8,128)(2,1)} %shard_map.118) | data formatting | bytes 1048576
  (2 shorter events, 0.0 us)

commit v3 on v2

--- a/solution.py
+++ b/solution.py
@@ -260,7 +260,8 @@
 
 
 MESH = pl.DeviceIdType.MESH
-A_CHUNKS = 2
+A_CHUNKS = 4
+W_CHUNKS = 4
 OUT_CHUNKS = 2
 LANES = 128
 
@@ -382,8 +383,15 @@
     def home(zz, yy):
         return pl.multiple_of((zz * 2 + yy) * depth, depth)
 
-    def wide(ref, start):
-        return ref.at[pl.ds(start, depth), pl.ds(0, three)]
+    fine, fine_kv = depth // W_CHUNKS, half // W_CHUNKS
+
+    def pieces(ref, start, cc, j):
+        low = pl.multiple_of(start + j * fine, fine)
+        low_kv = pl.multiple_of(start + cc * half + j * fine_kv, fine_kv)
+        return [
+            ref.at[pl.ds(low, fine), pl.ds(0, three)],
+            ref.at[pl.ds(low_kv, fine_kv), pl.ds(three, width)],
+        ]
 
     def narrow(ref, start, cc):
         return ref.at[pl.ds(pl.multiple_of(start + cc * half, half), half), pl.ds(three, width)]
@@ -416,41 +424,24 @@
                 for i, b in enumerate(w_targets(ref, start, c)):
                     remote(b, b, w1_sem, kind * 4 + i, across_x).wait_recv()
 
-    def second_local():
+    def staged(src_t):
+        return pl.multiple_of(src_t * depth, depth)
+
+    def second(src_t, j):
         return [
-            remote(a, b, w2_sem, z * 4 + i, at(t, y, t), t * 4 + i)
-            for i, (a, b) in enumerate(zip(w_sources(t), w_targets(w_all, home(z, y), c)))
-        ]
-
-    def second_staged(src_t):
-        start = pl.multiple_of(src_t * depth, depth)
-        return [
-            remote(a, b, w2_sem, z * 4 + i, at(src_t, y, t), src_t * 4 + i)
-            for a, b, i in (
-                (wide(stage, start), wide(w_all, home(z, y)), 0),
-                (narrow(stage, start, c), narrow(w_all, home(z, y), c), 3),
+            remote(a, b, w2_sem, (z * W_CHUNKS + j) * 2 + i, at(src_t, y, t), (src_t * W_CHUNKS + j) * 2 + i)
+            for i, (a, b) in enumerate(
+                zip(pieces(stage, staged(src_t), c, j), pieces(w_all, home(z, y), c, j))
             )
         ]
 
-    def second_arrival(from_z):
-        start = home(from_z, y)
-
-        @pl.when(t == z)
-        def _():
-            for i, ref in enumerate(w_targets(w_all, start, c)):
-                remote(ref, ref, w2_sem, from_z * 4 + i, across_x).wait_recv()
-
-        @pl.when(t != z)
-        def _():
-            for ref, i in ((wide(w_all, start), 0), (narrow(w_all, start, c), 3)):
-                remote(ref, ref, w2_sem, from_z * 4 + i, across_x).wait_recv()
-
-    def third(from_z, arrival=False):
-        start = home(from_z, 1 - y if arrival else y)
-        return [
-            remote(ref, ref, w3_sem, from_z * 2 + i, across_y)
-            for i, ref in enumerate((narrow(w_all, start, c), wide(w_all, start)))
-        ]
+    def second_arrival(from_z, j):
+        for i, ref in enumerate(pieces(w_all, home(from_z, y), c, j)):
+            remote(ref, ref, w2_sem, (from_z * W_CHUNKS + j) * 2 + i, across_x).wait_recv()
+
+    def third(from_z, j, i, arrival=False):
+        ref = pieces(w_all, home(from_z, 1 - y if arrival else y), c, j)[i]
+        return remote(ref, ref, w3_sem, (from_z * W_CHUNKS + j) * 2 + i, across_y)
 
     def to_share(from_z, own, arrival=False):
         ref = narrow(w_all, home(from_z, y if own else 1 - y), 1 - c if arrival else c)
@@ -469,10 +460,13 @@
         pltpu.make_async_copy(a, b, local_sem.at[4 + i])
         for i, (a, b) in enumerate(zip((out_attn, out_conv), out_copies(y)))
     ]
-    own_loads = [
-        pltpu.make_async_copy(a, b, local_sem.at[i])
-        for i, (a, b) in enumerate(zip(w_sources(t)[:3], w_targets(w_all, home(z, y), c)))
-    ]
+
+    def own_loads(ref, start):
+        return [
+            pltpu.make_async_copy(a, b, local_sem.at[i])
+            for i, (a, b) in enumerate(zip(w_sources(t)[:3], w_targets(ref, start, c)))
+        ]
+
 
     for chunk in range(A_CHUNKS):
         for way in range(2):
@@ -497,45 +491,43 @@
             small_copy(*args).start()
         small[...] = small_src[t]
 
+    for here, ref, start in ((t == z, w_all, home(z, y)), (t != z, stage, staged(t))):
+        @pl.when(here)
+        def _():
+            for copy in own_loads(ref, start):
+                copy.start()
+            ref[pl.ds(pl.multiple_of(start + c * half, half), half), three : three + width] = w_kv[t]
+
     first_all(2, partner, tp, lambda copy: copy.start())
     first_all(0, across_x, tx, lambda copy: copy.start())
     first_all(1, diagonal, td, lambda copy: copy.start())
-    for copy in outs:
+    for copy in outs + out_loads:
         copy.start()
-    for copy in out_loads:
-        copy.start()
-
-    @pl.when(t == z)
-    def _():
-        for copy in own_loads:
-            copy.start()
-        start = pl.multiple_of(home(z, y) + c * half, half)
-        w_all[pl.ds(start, half), three : three + width] = w_kv[t]
-        for copy in own_loads:
-            copy.wait()
+    for here, ref, start in ((t == z, w_all, home(z, y)), (t != z, stage, staged(t))):
+        @pl.when(here)
+        def _():
+            for copy in own_loads(ref, start):
+                copy.wait()
 
     def toward(target, way):
         return target > z if way == 0 else target < z
 
-    def send_second(way):
-        @pl.when(toward(t, way))
-        def _():
-            for copy in second_local():
-                copy.start()
-
-        for src_t in (tp, tx, td):
-            @pl.when(toward(src_t, way))
-            def _():
-                for copy in second_staged(src_t):
-                    copy.start()
-
-    def first_arrivals():
-        first_arrival(2, tp)
-        first_arrival(0, tx)
-        first_arrival(1, td)
-
-    def chain_step(distance):
-        for chunk in range(A_CHUNKS):
+    def next_to(target, way):
+        return target == (z + 1 if way == 0 else z - 1)
+
+    def send_second(way, sources, near):
+        for j in range(W_CHUNKS):
+            for src_t in sources:
+                beside = next_to(src_t, way)
+                beyond = jnp.logical_and(toward(src_t, way), jnp.logical_not(beside))
+
+                @pl.when(beside if near else beyond)
+                def _():
+                    for copy in second(src_t, j):
+                        copy.start()
+
+    def chain_step(distance, chunks=range(A_CHUNKS)):
+        for chunk in chunks:
             for way in range(2):
                 @pl.when(exists(way, distance))
                 def _():
@@ -556,40 +548,35 @@
                     sideways(way, distance, chunk, True).wait_recv()
                     to_partner(way, distance, chunk, 1).start()
 
-    def settle(from_z):
-        to_share(from_z, 1).start()
-        for copy in third(from_z):
-            copy.start()
-
-    def plane_step(distance):
-        for way in range(2):
-            @pl.when(exists(way, distance))
-            def _():
-                second_arrival(origin(way, distance))
-                settle(origin(way, distance))
+    def settle(from_z, j):
+        for i in range(2):
+            third(from_z, j, i).start()
+        if j == W_CHUNKS - 1:
+            to_share(from_z, 1).start()
+
+    def block_step(from_z, j):
+        second_arrival(from_z, j)
+        settle(from_z, j)
 
     ends = jnp.logical_or(z == 0, z == planes - 1)
-
-    @pl.when(ends)
-    def _():
-        first_arrivals()
-        for way in range(2):
-            send_second(way)
 
     for k in range(1, planes):
         normalise(lax.rem(t + k, planes) * piece, piece)
-    for distance in range(1, planes - 1):
+    first_arrival(2, tp)
+    chain_step(1)
+    for way in range(2):
+        send_second(way, (t, tp), True)
+
+    first_arrival(0, tx)
+    first_arrival(1, td)
+    for way in range(2):
+        send_second(way, (tx, td), True)
+        send_second(way, (t, tp, tx, td), False)
+
+    for j in range(W_CHUNKS):
+        settle(z, j)
+    for distance in range(2, planes - 1):
         chain_step(distance)
-        if distance == 1:
-            @pl.when(jnp.logical_not(ends))
-            def _():
-                first_arrivals()
-
-            settle(z)
-        for way in range(2):
-            @pl.when(jnp.logical_and(jnp.logical_not(ends), z == (distance if way == 0 else planes - 1 - distance)))
-            def _():
-                send_second(way)
 
     row = lax.broadcasted_iota(jnp.int32, (block, LANES), 0)
     for zz in range(planes):
@@ -598,15 +585,18 @@
         cosine[here, :] = jnp.cos(angle)
         sine[here, :] = jnp.sin(angle)
 
-    chain_step(planes - 1)
-    plane_step(1)
-    sideways_step(1)
-    plane_step(2)
-    for distance in range(2, planes):
-        sideways_step(distance)
-    for distance in range(3, planes):
-        plane_step(distance)
-    for distance in range(1, planes):
+    ahead = 1 - 2 * (z // (planes // 2))
+    end = (z // (planes // 2)) * (planes - 1)
+    middle = jnp.logical_not(ends)
+
+    blocks_from = [
+        z,
+        jnp.where(middle, end, z + ahead),
+        jnp.where(middle, planes - 1 - z, z + 2 * ahead),
+        jnp.where(middle, planes - 1 - end, z + 3 * ahead),
+    ]
+
+    def tokens_here(distance):
         for chunk in range(A_CHUNKS):
             for way in range(2):
                 @pl.when(exists(way, distance))
@@ -614,40 +604,75 @@
                     for far in range(2):
                         to_partner(way, distance, chunk, far, True).wait_recv()
 
-    ahead = 1 - 2 * (z // (planes // 2))
-    tall = rows // 2
+    first_row = (z // (planes // 2)) * block
+    last_row = (planes - 1) * block - end * block
 
     def multiply(from_z, yy, fresh):
-        start = home(from_z, yy)
-        cols = pl.ds(start, depth)
-
-        @pl.loop(0, 2)
+        cols = pl.ds(home(from_z, yy), depth)
+
+        @pl.loop(0, planes - 1)
         def _(i):
-            here = pl.ds(pl.multiple_of(i * tall, tall), tall)
+            here = pl.ds(pl.multiple_of(first_row + i * block, block), block)
             value = jnp.dot(rows_all[here, cols], w_all[cols, :], preferred_element_type=f32)
             if fresh:
                 acc[here, :] = value
             else:
                 acc[here, :] += value
 
-    to_share(z, 1, True).wait_recv()
-    multiply(z, y, True)
-
-    @pl.loop(1, planes)
-    def _(k):
-        from_z = lax.rem(z + k * ahead + planes, planes)
-        to_share(from_z, 1, True).wait_recv()
-        multiply(from_z, y, False)
-
-    @pl.loop(0, planes)
-    def _(k):
-        from_z = lax.rem(z + k * ahead + planes, planes)
-        narrow_copy, wide_copy = third(from_z, True)
-        narrow_copy.wait_recv()
-        to_share(from_z, 0).start()
-        wide_copy.wait_recv()
-        to_share(from_z, 0, True).wait_recv()
-        multiply(from_z, 1 - y, False)
+    def multiply_own(pair):
+        for k in pair:
+            to_share(blocks_from[k], 1, True).wait_recv()
+            if k == 0:
+                multiply(blocks_from[0], y, True)
+        if 0 not in pair:
+            multiply(blocks_from[pair[0]], y, False)
+        multiply(blocks_from[pair[1]], y, False)
+
+    def share_other(pair):
+        for k in pair:
+            for j in range(W_CHUNKS):
+                third(blocks_from[k], j, 1, True).wait_recv()
+            to_share(blocks_from[k], 0).start()
+
+    def multiply_other(pair):
+        for k in pair:
+            for j in range(W_CHUNKS):
+                third(blocks_from[k], j, 0, True).wait_recv()
+            to_share(blocks_from[k], 0, True).wait_recv()
+
+        @pl.loop(0, 2)
+        def _(i):
+            multiply(jnp.where(i == 0, blocks_from[pair[0]], blocks_from[pair[1]]), 1 - y, False)
+
+    for j in range(W_CHUNKS):
+        block_step(blocks_from[1], j)
+    sideways_step(1)
+    for j in range(W_CHUNKS):
+        block_step(blocks_from[2], j)
+        block_step(blocks_from[3], j)
+        if j == 1:
+            sideways_step(2)
+        if j == 2:
+            chain_step(planes - 1, range(A_CHUNKS // 4))
+            share_other((0, 1))
+            for distance in range(1, planes - 1):
+                tokens_here(distance)
+            multiply_own((0, 1))
+            multiply_other((0, 1))
+            chain_step(planes - 1, range(A_CHUNKS // 4, A_CHUNKS // 2))
+    chain_step(planes - 1, range(A_CHUNKS // 2, A_CHUNKS))
+    multiply_own((2, 3))
+    share_other((2, 3))
+    sideways_step(planes - 1)
+    multiply_other((2, 3))
+
+    tokens_here(planes - 1)
+    here = pl.ds(pl.multiple_of(last_row, block), block)
+
+    @pl.loop(0, 2)
+    def _(i):
+        cols = pl.ds(pl.multiple_of(i * 2 * width, 2 * width), 2 * width)
+        acc[here, cols] = jnp.dot(rows_all[here, :], w_all[:, cols], preferred_element_type=f32)
 
     lane = lax.broadcasted_iota(jnp.int32, (block, LANES), 1)
     low = lax.rem(lane, HEAD) < HEAD // 2
@@ -743,6 +768,12 @@
             before = pl.multiple_of(zz * block + (b - 1) * WINDOW, WINDOW)
             attend(start, kv_b[pl.ds(before, 2 * WINDOW), :], inside)
 
+    def attend_first(zz):
+        start = pl.multiple_of(zz * block, block)
+        keys = jnp.concatenate([kv_rim[zz], kv_b[pl.ds(start, WINDOW), :]], axis=0)
+        began = jnp.logical_or(zz * 2 + y > 0, col_s >= WINDOW)
+        attend(start, keys, jnp.logical_and(inside, began))
+
     for zz in range(planes):
         if zz < planes - 1:
             halo_arrival(1, zz).wait_recv()
@@ -799,13 +830,6 @@
             if zz == planes - 1:
                 halo_arrival(0, zz).wait_recv()
 
-    @pl.loop(0, planes)
-    def _(zz):
-        start = pl.multiple_of(zz * block, block)
-        keys = jnp.concatenate([kv_rim[zz], kv_b[pl.ds(start, WINDOW), :]], axis=0)
-        began = jnp.logical_or(zz * 2 + y > 0, col_s >= WINDOW)
-        attend(start, keys, jnp.logical_and(inside, began))
-
     def region(kind, r, tt):
         start = pl.multiple_of(r * block, block)
         return act.at[pl.ds(start, block), columns(kind, tt)]
@@ -821,9 +845,14 @@
 
     near = z // (planes // 2)
     order = [(1 - near) * (planes - 1 - j) + near * j for j in range(planes)]
+    def send_out(kind, r):
+        cross(kind, r).start()
+        hand(kind, r, 0).start()
+
     for r in order:
-        cross(0, r).start()
-        hand(0, r, 0).start()
+        attend_first(r)
+        if r is order[0]:
+            send_out(0, r)
     for g in peers:
         ref = stats_all.at[g]
         pltpu.make_async_remote_copy(
@@ -852,23 +881,6 @@
             scaled = (filtered[here, :] - mean_col) * rate_col * small[32:33, :]
             act[here, columns(1, t)] = (scaled / (1.0 + jnp.exp(-scaled))).astype(act.dtype)
 
-    for r in order:
-        normed_out(r)
-        cross(1, r).start()
-        hand(1, r, 0).start()
-    for copy in out_loads:
-        copy.wait()
-    for copy in outs:
-        copy.wait_recv()
-    for kind in range(2):
-        for r in order:
-            cross(kind, r, True).wait_recv()
-            hand(kind, r, 1).start()
-    for kind in range(2):
-        for r in order:
-            for far in range(2):
-                hand(kind, r, far, True).wait_recv()
-
     out_step = block // OUT_CHUNKS
     columns_out = mixed.shape[1]
     tile_out = min(256, columns_out)
@@ -886,7 +898,7 @@
         source = into if arrival else outgoing.at[r, rows_h]
         return remote(source, into, r_sem, index, across_y if arrival else at(z + 1 if way == 0 else z - 1, y, t))
 
-    for distance in range(planes - 1, 0, -1):
+    def pass_sums(distance):
         for h in range(OUT_CHUNKS):
             rows_h = pl.ds(h * out_step, out_step)
             for way in range(2):
@@ -917,6 +929,31 @@
 
                     travel(way, r, h).start()
 
+    def gathered(js):
+        for j in js:
+            for kind in range(2):
+                cross(kind, order[j], True).wait_recv()
+                hand(kind, order[j], 1).start()
+        for j in js:
+            for kind in range(2):
+                for far in range(2):
+                    hand(kind, order[j], far, True).wait_recv()
+
+    for r in order:
+        normed_out(r)
+        send_out(1, r)
+        if r is not order[0]:
+            send_out(0, r)
+    for copy in out_loads:
+        copy.wait()
+    for copy in outs:
+        copy.wait_recv()
+    gathered([0])
+    pass_sums(planes - 1)
+    gathered(range(1, planes))
+    for distance in range(planes - 2, 0, -1):
+        pass_sums(distance)
+
     for h in range(OUT_CHUNKS):
         rows_h = pl.ds(h * out_step, out_step)
 
@@ -966,20 +1003,17 @@
     first_all(0, across_x, tx, lambda copy: copy.wait_send())
     first_all(1, diagonal, td, lambda copy: copy.wait_send())
 
-    @pl.when(t != z)
-    def _():
-        for copy in second_local():
-            copy.wait_send()
-
-    for src_t in (tp, tx, td):
+    for src_t in (t, tp, tx, td):
         @pl.when(src_t != z)
         def _():
-            for copy in second_staged(src_t):
-                copy.wait_send()
+            for j in range(W_CHUNKS):
+                for copy in second(src_t, j):
+                    copy.wait_send()
 
     for zz in range(planes):
-        for copy in third(zz):
-            copy.wait_send()
+        for j in range(W_CHUNKS):
+            for i in range(2):
+                third(zz, j, i).wait_send()
         for own in range(2):
             to_share(zz, own).wait_send()
     for distance in range(planes):
@@ -1043,7 +1077,7 @@
     tiles = rows // LANES
     chunks = 2 * planes * A_CHUNKS
     counts = [
-        chunks, chunks, 2 * chunks, 12, 4 * planes, 2 * planes, 2 * planes, 2, 3,
+        chunks, chunks, 2 * chunks, 12, 2 * planes * W_CHUNKS, 2 * planes * W_CHUNKS, 2 * planes, 2, 3,
         2 * planes, size, 2 * planes, 4 * planes, 2 * planes * OUT_CHUNKS,
     ]
     sems = [dma((n,)) for n in counts for _ in range(2)]

time: 175 us -> 152 us (0.87)
  Pallas kernels: 171 us -> 149 us
    pallas_call x1, Pallas kernels: 171 us -> 149 us  [planned_per_device(): pl.pallas_call(functools.partial(layer_kernel, planes, CONV), out_shape=j...]
where the time goes in v3:
time: 152 us; the launch traced here: 151 us
  Pallas kernels  149 us (98%)
  local copies, waits for them, and re-layouts  2.47 us (2%)
    pallas_call x1, Pallas kernels, planned_per_device(): pl.pallas_call(functools.partial(layer_kernel, planes, CONV), out_shape=j...  149 us

profile of v3, /device:TPU:0, one launch (start us, length us, event | category | flops | bytes accessed | tf_op | source)
XLA Modules:
  0.0 151.1 jit_solution(9298155039115365160)
XLA Ops:
  0.0 0.6 broadcast_in_dim_tile.3.refs_2_
  0.6 148.6 %shard_map.118 = bf16[256,1024]{1,0:T(8,128)(2,1)} custom-call(bf16[256,4096]{1,0:T(8,128)(2,1)} %refs_0_.1, f32[1,4096]{1,0:T(1,128)} %bitcast.3, f32[1,128]{1,0:T(1,128)} %broadcast_in_dim_tile.3.refs_2_, bf16[512,128]{1,0:T(8,128)(2,1)} %refs_3_.1, bf16[512,128]{1,0:T(8,128)(2,1)} %refs_4_.1, bf16[31,512]{1,0:T(8,128)(2,1)} %refs_5_.1, f32[1,512]{1,0:T(1,128)} %bitcast.4, ...), custom_call_target="tpu_custom_call" | custom-call | tf_op jit(solution)/shard_map/pallas_call | solution.py:1084
  149.2 1.9 %copy.14 = bf16[256,1024]{1,0:T(8,128)(2,1)} copy(bf16[256,1024]{1,0:T(8,128)(2,1)} %shard_map.118) | data formatting | bytes 1048576
  (2 shorter events, 0.0 us)

commit v4 on v3

--- a/solution.py
+++ b/solution.py
@@ -262,20 +262,28 @@
 MESH = pl.DeviceIdType.MESH
 A_CHUNKS = 4
 W_CHUNKS = 4
-OUT_CHUNKS = 2
+OUT_CHUNKS = 4
 LANES = 128
 
 
-def remote(src, dst, sems, index, target, send_index=None):
+def remote(src, dst, sems, index, target):
     send_sem, recv_sem = sems
     return pltpu.make_async_remote_copy(
         src_ref=src,
         dst_ref=dst,
-        send_sem=send_sem.at[index if send_index is None else send_index],
+        send_sem=send_sem.at[0],
         recv_sem=recv_sem.at[index],
         device_id=target,
         device_id_type=MESH,
     )
+
+
+def all_sent(ref, sems, target):
+    remote(ref, ref, sems, 0, target).wait_send()
+
+
+def all_here(ref, sems, index, target):
+    remote(ref, ref, sems, index, target).wait_recv()
 
 
 def layer_kernel(planes, channels, *refs):
@@ -284,11 +292,11 @@
     mixed = refs[13]
     (rows_all, w_all, stage, w_kv, small_src, small) = refs[14:20]
     (acc, cosine, sine, q_b, kv_b, kv_rim, gated, gated_rim, extended, filtered) = refs[20:30]
-    (act, weights, stats, stats_all, moments, in_up, in_down, outgoing) = refs[30:38]
-    local_sem = refs[38]
-    pairs = [(refs[39 + 2 * i], refs[40 + 2 * i]) for i in range((len(refs) - 39) // 2)]
+    (act, weights, stats, stats_all, moments, incoming, outgoing) = refs[30:37]
+    local_sem = refs[37]
+    pairs = [(refs[38 + 2 * i], refs[39 + 2 * i]) for i in range((len(refs) - 38) // 2)]
     (a_sem, ax_sem, ac_sem, w1_sem, w2_sem, w3_sem, kc_sem, o_sem, small_sem) = pairs[:9]
-    (halo_sem, s_sem, x_sem, c_sem, r_sem) = pairs[9:14]
+    (halo_sem, s_sem, e_sem, x_sem, c_sem, r_sem) = pairs[9:15]
 
     s, t = lax.axis_index("sp"), lax.axis_index("tp")
     z, y, x, c = s // 2, s % 2, t // 2, t % 2
@@ -374,11 +382,10 @@
         index = (way * planes + distance) * A_CHUNKS + chunk
         return remote(ref, ref, ax_sem, index, across_x)
 
-    def to_partner(way, distance, chunk, far, arrival=False):
-        tt = (td if far else tp) if arrival else (tx if far else t)
+    def to_partner(way, distance, chunk, far):
+        tt = tx if far else t
         ref = rows_of(origin(way, distance), tt, chunk)
-        index = ((way * planes + distance) * A_CHUNKS + chunk) * 2 + far
-        return remote(ref, ref, ac_sem, index, partner)
+        return remote(ref, ref, ac_sem, way * planes + distance, partner)
 
     def home(zz, yy):
         return pl.multiple_of((zz * 2 + yy) * depth, depth)
@@ -411,46 +418,55 @@
         ):
             @pl.when(here)
             def _():
-                for i, (a, b) in enumerate(zip(w_sources(tt), w_targets(ref, start, tt % 2))):
-                    what(remote(a, b, w1_sem, kind * 4 + i, target))
-
-    def first_arrival(kind, src_t):
-        for here, ref, start in (
-            (src_t == z, w_all, home(z, y)),
-            (src_t != z, stage, pl.multiple_of(src_t * depth, depth)),
-        ):
-            @pl.when(here)
-            def _():
-                for i, b in enumerate(w_targets(ref, start, c)):
-                    remote(b, b, w1_sem, kind * 4 + i, across_x).wait_recv()
+                for a, b in zip(w_sources(tt), w_targets(ref, start, tt % 2)):
+                    what(remote(a, b, w1_sem, kind, target))
+
+    block_rows = 3 * depth // 4 + half // 4
+
+    def first_arrival(kind):
+        all_here(w_all.at[pl.ds(0, block_rows)], w1_sem, kind, across_x)
 
     def staged(src_t):
         return pl.multiple_of(src_t * depth, depth)
 
     def second(src_t, j):
         return [
-            remote(a, b, w2_sem, (z * W_CHUNKS + j) * 2 + i, at(src_t, y, t), (src_t * W_CHUNKS + j) * 2 + i)
-            for i, (a, b) in enumerate(
-                zip(pieces(stage, staged(src_t), c, j), pieces(w_all, home(z, y), c, j))
-            )
+            remote(a, b, w2_sem, z * W_CHUNKS + j, at(src_t, y, t))
+            for a, b in zip(pieces(stage, staged(src_t), c, j), pieces(w_all, home(z, y), c, j))
         ]
 
     def second_arrival(from_z, j):
-        for i, ref in enumerate(pieces(w_all, home(from_z, y), c, j)):
-            remote(ref, ref, w2_sem, (from_z * W_CHUNKS + j) * 2 + i, across_x).wait_recv()
-
-    def third(from_z, j, i, arrival=False):
-        ref = pieces(w_all, home(from_z, 1 - y if arrival else y), c, j)[i]
-        return remote(ref, ref, w3_sem, (from_z * W_CHUNKS + j) * 2 + i, across_y)
+        all_here(w_all.at[pl.ds(0, block_rows // W_CHUNKS)], w2_sem, from_z * W_CHUNKS + j, across_x)
+
+    def third(from_z, j, i):
+        ref = pieces(w_all, home(from_z, y), c, j)[i]
+        return remote(ref, ref, w3_sem, from_z * 2 + i, across_y)
 
     def to_share(from_z, own, arrival=False):
         ref = narrow(w_all, home(from_z, y if own else 1 - y), 1 - c if arrival else c)
         return remote(ref, ref, kc_sem, from_z * 2 + own, partner)
 
-    def out_copies(yy):
-        low = pl.multiple_of(yy * group, group)
-        high = pl.multiple_of(part + yy * group, group)
-        return [weights.at[pl.ds(low, group)], weights.at[pl.ds(high, group)]]
+    ahead = 1 - 2 * (z // (planes // 2))
+    end = (z // (planes // 2)) * (planes - 1)
+    ends = jnp.logical_or(z == 0, z == planes - 1)
+    middle = jnp.logical_not(ends)
+
+    def out_copies(yy, side=0):
+        return [
+            weights.at[pl.ds(pl.multiple_of((2 * side + kind) * part + yy * group, group), group)]
+            for kind in range(2)
+        ]
+
+    end_outs = [
+        remote(a, b, o_sem, 2 + i, at(z + ahead, y, t))
+        for i, (a, b) in enumerate(zip((out_attn, out_conv), out_copies(y, 1)))
+    ]
+    half_group = group // 2
+
+    def end_across(i, arrival=False):
+        start = (2 + i // 2) * part + (1 - y if arrival else y) * group + (i % 2) * half_group
+        ref = weights.at[pl.ds(pl.multiple_of(start, half_group), half_group)]
+        return remote(ref, ref, o_sem, 4 + i, across_y)
 
     outs = [
         remote(a, b, o_sem, i, across_y)
@@ -473,13 +489,19 @@
             @pl.when(can_send(way, 0))
             def _():
                 chain(way, 0, chunk).start()
+
+    @pl.when(ends)
+    def _():
+        for copy in end_outs:
+            copy.start()
+
     small_to = [(partner, tp, 0), (across_x, tx, 1), (diagonal, td, 2)]
 
     def small_copy(target, tt, i):
         return pltpu.make_async_remote_copy(
             src_ref=small_src.at[tt],
             dst_ref=small,
-            send_sem=small_sem[0].at[i],
+            send_sem=small_sem[0].at[0],
             recv_sem=small_sem[1].at[0],
             device_id=target,
             device_id_type=MESH,
@@ -549,7 +571,7 @@
                     to_partner(way, distance, chunk, 1).start()
 
     def settle(from_z, j):
-        for i in range(2):
+        for i in (1, 0):
             third(from_z, j, i).start()
         if j == W_CHUNKS - 1:
             to_share(from_z, 1).start()
@@ -558,20 +580,19 @@
         second_arrival(from_z, j)
         settle(from_z, j)
 
-    ends = jnp.logical_or(z == 0, z == planes - 1)
-
     for k in range(1, planes):
         normalise(lax.rem(t + k, planes) * piece, piece)
-    first_arrival(2, tp)
+    first_arrival(2)
     chain_step(1)
     for way in range(2):
         send_second(way, (t, tp), True)
 
-    first_arrival(0, tx)
-    first_arrival(1, td)
+    first_arrival(0)
+    first_arrival(1)
     for way in range(2):
         send_second(way, (tx, td), True)
         send_second(way, (t, tp, tx, td), False)
+
 
     for j in range(W_CHUNKS):
         settle(z, j)
@@ -585,9 +606,11 @@
         cosine[here, :] = jnp.cos(angle)
         sine[here, :] = jnp.sin(angle)
 
-    ahead = 1 - 2 * (z // (planes // 2))
-    end = (z // (planes // 2)) * (planes - 1)
-    middle = jnp.logical_not(ends)
+    @pl.when(middle)
+    def _():
+        end_outs[0].wait_recv()
+        for i in range(2):
+            end_across(i).start()
 
     blocks_from = [
         z,
@@ -597,12 +620,10 @@
     ]
 
     def tokens_here(distance):
-        for chunk in range(A_CHUNKS):
-            for way in range(2):
-                @pl.when(exists(way, distance))
-                def _():
-                    for far in range(2):
-                        to_partner(way, distance, chunk, far, True).wait_recv()
+        for way in range(2):
+            @pl.when(exists(way, distance))
+            def _():
+                all_here(rows_all.at[pl.ds(0, 2 * piece)], ac_sem, way * planes + distance, partner)
 
     first_row = (z // (planes // 2)) * block
     last_row = (planes - 1) * block - end * block
@@ -630,14 +651,12 @@
 
     def share_other(pair):
         for k in pair:
-            for j in range(W_CHUNKS):
-                third(blocks_from[k], j, 1, True).wait_recv()
+            all_here(narrow(w_all, 0, 0), w3_sem, blocks_from[k] * 2 + 1, across_y)
             to_share(blocks_from[k], 0).start()
 
     def multiply_other(pair):
         for k in pair:
-            for j in range(W_CHUNKS):
-                third(blocks_from[k], j, 0, True).wait_recv()
+            all_here(w_all.at[pl.ds(0, depth), pl.ds(0, three)], w3_sem, blocks_from[k] * 2, across_y)
             to_share(blocks_from[k], 0, True).wait_recv()
 
         @pl.loop(0, 2)
@@ -661,6 +680,11 @@
             multiply_other((0, 1))
             chain_step(planes - 1, range(A_CHUNKS // 4, A_CHUNKS // 2))
     chain_step(planes - 1, range(A_CHUNKS // 2, A_CHUNKS))
+    @pl.when(middle)
+    def _():
+        end_outs[1].wait_recv()
+        end_across(2).start()
+
     multiply_own((2, 3))
     share_other((2, 3))
     sideways_step(planes - 1)
@@ -717,6 +741,10 @@
     @pl.when(t != z)
     def _():
         small_copy(partner, tp, 0).wait_recv()
+
+    @pl.when(middle)
+    def _():
+        end_across(3).start()
 
     lane_q = lax.broadcasted_iota(jnp.int32, (WINDOW, LANES), 1)
     lane_k = lax.broadcasted_iota(jnp.int32, (2 * WINDOW, LANES), 1)
@@ -756,17 +784,15 @@
             result = jnp.where(lane_q // HEAD == h, mixed_values[h * WINDOW : (h + 1) * WINDOW], result)
         act[pl.ds(first_row, WINDOW), columns(0, t)] = result.astype(act.dtype)
 
-    def columns(kind, tt):
-        return pl.ds(pl.multiple_of(kind * part + tt * width, width), width)
+    def columns(kind, tt, side=0):
+        return pl.ds(pl.multiple_of((2 * side + kind) * part + tt * width, width), width)
 
     blocks = block // WINDOW
 
-    @pl.loop(0, planes)
-    def _(zz):
+    for zz in range(planes):
         for b in range(1, blocks):
-            start = pl.multiple_of(zz * block + b * WINDOW, WINDOW)
-            before = pl.multiple_of(zz * block + (b - 1) * WINDOW, WINDOW)
-            attend(start, kv_b[pl.ds(before, 2 * WINDOW), :], inside)
+            start = zz * block + b * WINDOW
+            attend(start, kv_b[pl.ds(start - WINDOW, 2 * WINDOW), :], inside)
 
     def attend_first(zz):
         start = pl.multiple_of(zz * block, block)
@@ -793,9 +819,12 @@
         def _(i):
             base = pl.multiple_of(i * strip, strip)
             window = extended[zz, pl.ds(base, strip + 32), :]
-            total = window[2 : 2 + strip] * small[0:1, :]
-            for k in range(1, KSIZE):
-                total = total + window[2 + k : 2 + k + strip] * small[k : k + 1, :]
+            total = jnp.zeros((strip, width), f32)
+            for shift in range(8):
+                moved = window[shift : shift + strip + 24] if shift else window
+                for k in range((shift - 2) % 8, KSIZE, 8):
+                    low = 2 + k - shift
+                    total = total + moved[low : low + strip] * small[k : k + 1, :]
             filtered[pl.ds(pl.multiple_of(zz * block + base, strip), strip), :] = total
 
     tiles = rows // LANES
@@ -811,8 +840,8 @@
         return pltpu.make_async_remote_copy(
             src_ref=stats,
             dst_ref=stats_all.at[mine],
-            send_sem=s_sem[0].at[k],
-            recv_sem=s_sem[1].at[mine],
+            send_sem=s_sem[0].at[0],
+            recv_sem=s_sem[1].at[0],
             device_id=at(g // planes, y, g % planes),
             device_id_type=MESH,
         )
@@ -830,39 +859,55 @@
             if zz == planes - 1:
                 halo_arrival(0, zz).wait_recv()
 
-    def region(kind, r, tt):
+    def region(kind, r, tt, side):
         start = pl.multiple_of(r * block, block)
-        return act.at[pl.ds(start, block), columns(kind, tt)]
-
-    def cross(kind, r, arrival=False):
-        ref = region(kind, r, tx if arrival else t)
-        return remote(ref, ref, x_sem, kind * planes + r, across_x)
-
-    def hand(kind, r, far, arrival=False):
-        tt = (td if far else tp) if arrival else (tx if far else t)
-        ref = region(kind, r, tt)
-        return remote(ref, ref, c_sem, (kind * planes + r) * 2 + far, partner)
+        return act.at[pl.ds(start, block), columns(kind, tt, side)]
+
+    def cross(kind, r, side, arrival=False):
+        ref = region(kind, r, tx if arrival else t, side)
+        return remote(ref, ref, x_sem, (side * 2 + kind) * planes + r, across_x)
+
+    def hand(kind, r, side, far):
+        ref = region(kind, r, tx if far else t, side)
+        return remote(ref, ref, c_sem, side * planes + r, partner)
+
+    def send_out(kind, r, side=0):
+        cross(kind, r, side).start()
+        hand(kind, r, side, 0).start()
 
     near = z // (planes // 2)
     order = [(1 - near) * (planes - 1 - j) + near * j for j in range(planes)]
-    def send_out(kind, r):
-        cross(kind, r).start()
-        hand(kind, r, 0).start()
-
-    for r in order:
-        attend_first(r)
-        if r is order[0]:
-            send_out(0, r)
-    for g in peers:
-        ref = stats_all.at[g]
-        pltpu.make_async_remote_copy(
-            src_ref=ref,
-            dst_ref=ref,
-            send_sem=s_sem[0].at[0],
-            recv_sem=s_sem[1].at[g],
-            device_id=partner,
-            device_id_type=MESH,
-        ).wait_recv()
+
+    def inward(kind, j):
+        source = region(kind, order[j], t, 0)
+        return remote(source, region(kind, order[j], t, 1), e_sem, kind * planes + j, at(z + ahead, y, t))
+
+    def pass_in(kind, j):
+        inward(kind, j).wait_recv()
+        send_out(kind, order[j], 1)
+
+    for pair in ((0, 1), (2, 3)):
+        for j in pair:
+            attend_first(order[j])
+
+        @pl.when(ends)
+        def _():
+            for j in pair:
+                if j < planes - 1:
+                    inward(0, j).start()
+
+        @pl.when(middle)
+        def _():
+            for j in pair:
+                if j < 2:
+                    send_out(0, order[j])
+
+    @pl.when(middle)
+    def _():
+        pass_in(0, 0)
+        pass_in(0, 1)
+
+    all_here(stats_all.at[pl.ds(0, size - 1)], s_sem, 0, partner)
     total = stats_all[0]
     for g in range(1, size):
         total = total + stats_all[g]
@@ -881,169 +926,150 @@
             scaled = (filtered[here, :] - mean_col) * rate_col * small[32:33, :]
             act[here, columns(1, t)] = (scaled / (1.0 + jnp.exp(-scaled))).astype(act.dtype)
 
-    out_step = block // OUT_CHUNKS
-    columns_out = mixed.shape[1]
-    tile_out = min(256, columns_out)
-
-    def partial(r, h, tile):
-        start = pl.multiple_of(r * block + h * out_step, out_step)
-        cols = pl.ds(pl.multiple_of(tile * tile_out, tile_out), tile_out)
-        value = jnp.dot(act[pl.ds(start, out_step), :], weights[:, cols], preferred_element_type=f32)
-        return value, cols
-
-    def travel(way, r, h, arrival=False):
-        rows_h = pl.ds(h * out_step, out_step)
-        into = (in_up if way == 0 else in_down).at[r, rows_h]
-        index = (way * planes + r) * OUT_CHUNKS + h
-        source = into if arrival else outgoing.at[r, rows_h]
-        return remote(source, into, r_sem, index, across_y if arrival else at(z + 1 if way == 0 else z - 1, y, t))
-
-    def pass_sums(distance):
-        for h in range(OUT_CHUNKS):
-            rows_h = pl.ds(h * out_step, out_step)
-            for way in range(2):
-                r = z + distance if way == 0 else z - distance
-                there = r < planes if way == 0 else r >= 0
-                more = z > 0 if way == 0 else z < planes - 1
-                into = in_up if way == 0 else in_down
-
-                @pl.when(jnp.logical_and(there, jnp.logical_not(more)))
-                def _():
-                    @pl.loop(0, columns_out // tile_out)
-                    def _(tile):
-                        value, cols = partial(r, h, tile)
-                        outgoing[r, rows_h, cols] = value.astype(outgoing.dtype)
-
-                    travel(way, r, h).start()
-
-                @pl.when(jnp.logical_and(there, more))
-                def _():
-                    travel(way, r, h, True).wait_recv()
-
-                    @pl.loop(0, columns_out // tile_out)
-                    def _(tile):
-                        value, cols = partial(r, h, tile)
-                        outgoing[r, rows_h, cols] = (value + into[r, rows_h, cols].astype(f32)).astype(
-                            outgoing.dtype
-                        )
-
-                    travel(way, r, h).start()
-
-    def gathered(js):
-        for j in js:
+    out_step = mixed.shape[1] // OUT_CHUNKS
+
+    def gathered(j, sides):
+        for side in sides:
             for kind in range(2):
-                cross(kind, order[j], True).wait_recv()
-                hand(kind, order[j], 1).start()
-        for j in js:
-            for kind in range(2):
-                for far in range(2):
-                    hand(kind, order[j], far, True).wait_recv()
-
-    for r in order:
+                cross(kind, order[j], side, True).wait_recv()
+                hand(kind, order[j], side, 1).start()
+        for side in sides:
+            ref = act.at[pl.ds(0, block), pl.ds(0, 4 * width)]
+            all_here(ref, c_sem, side * planes + order[j], partner)
+
+    def out_columns(h):
+        return pl.ds(pl.multiple_of(h * out_step, out_step), out_step)
+
+    def travel(slot, h, toward_z):
+        return remote(
+            outgoing.at[slot, :, out_columns(h)],
+            incoming.at[slot, :, out_columns(h)],
+            r_sem,
+            slot * OUT_CHUNKS + h,
+            at(toward_z, y, t),
+        )
+
+    def outputs(j, h, deep):
+        start = pl.multiple_of(order[j] * block, block)
+        deep_rows = slice(0, (4 if deep else 2) * part)
+        return jnp.dot(
+            act[pl.ds(start, block), deep_rows], weights[deep_rows, out_columns(h)], preferred_element_type=f32
+        )
+
+    def send_sums(j, deep, came, slot, toward_z):
+        @pl.loop(0, OUT_CHUNKS)
+        def _(h):
+            value = outputs(j, h, deep)
+            if came is not None:
+                travel(came, h, across_z).wait_recv()
+                value = value + incoming[came, :, out_columns(h)].astype(f32)
+            outgoing[slot, :, out_columns(h)] = value.astype(outgoing.dtype)
+            travel(slot, h, toward_z).start()
+
+    def finish(j, deep, came):
+        @pl.loop(0, OUT_CHUNKS)
+        def _(h):
+            value = outputs(j, h, deep)
+            travel(came, h, across_z).wait_recv()
+            mixed[:, out_columns(h)] = value + incoming[came, :, out_columns(h)].astype(f32)
+
+    across_z = z + ahead
+
+    for j, r in enumerate(order):
         normed_out(r)
-        send_out(1, r)
-        if r is not order[0]:
-            send_out(0, r)
+
+        @pl.when(ends)
+        def _():
+            if j < planes - 1:
+                inward(1, j).start()
+            else:
+                send_out(0, r)
+                send_out(1, r)
+
+        if j == 0:
+            @pl.when(middle)
+            def _():
+                send_out(1, r)
+
     for copy in out_loads:
         copy.wait()
     for copy in outs:
         copy.wait_recv()
-    gathered([0])
-    pass_sums(planes - 1)
-    gathered(range(1, planes))
-    for distance in range(planes - 2, 0, -1):
-        pass_sums(distance)
-
-    for h in range(OUT_CHUNKS):
-        rows_h = pl.ds(h * out_step, out_step)
-
-        @pl.when(z > 0)
-        def _():
-            travel(0, z, h, True).wait_recv()
-
-        @pl.when(z < planes - 1)
-        def _():
-            travel(1, z, h, True).wait_recv()
-
-        @pl.loop(0, columns_out // tile_out)
-        def _(tile):
-            value, cols = partial(z, h, tile)
-            below = in_up[z, rows_h, cols].astype(f32)
-            above = in_down[z, rows_h, cols].astype(f32)
-            value = value + jnp.where(z > 0, below, 0.0) + jnp.where(z < planes - 1, above, 0.0)
-            mixed[rows_h, cols] = value.astype(mixed.dtype)
+
+    @pl.when(middle)
+    def _():
+        for i in range(4):
+            end_across(i, True).wait_recv()
+
+    @pl.when(middle)
+    def _():
+        pass_in(1, 0)
+        send_out(1, order[1])
+        gathered(0, (0, 1))
+        send_sums(0, True, None, 0, across_z)
+
+    @pl.when(middle)
+    def _():
+        pass_in(1, 1)
+        for kind in range(2):
+            send_out(kind, order[3])
+        gathered(1, (0, 1))
+        send_sums(1, True, None, 1, across_z)
+
+    @pl.when(middle)
+    def _():
+        for kind in range(2):
+            send_out(kind, order[2])
+            pass_in(kind, 2)
+        gathered(3, (0,))
+        send_sums(3, False, 0, 2, z - ahead)
+
+    @pl.when(middle)
+    def _():
+        gathered(2, (0, 1))
+        finish(2, True, 1)
+
+    @pl.when(ends)
+    def _():
+        gathered(3, (0,))
+        finish(3, False, 2)
 
     @pl.when(t == z)
     def _():
-        for args in small_to:
-            small_copy(*args).wait_send()
-
-    @pl.when(y == 0)
-    def _():
-        for kind in range(2):
-            halo(kind, planes - 1).wait_send()
-
-    @pl.when(y == 1)
-    def _():
-        for kind in range(2):
-            halo(kind, planes - 1).wait_send()
-
-    for zz in range(planes - 1):
-        for kind in range(2):
-            halo(kind, zz).wait_send()
+        all_sent(small_src.at[pl.ds(0, 3)], small_sem, partner)
 
     @pl.when(y == 0)
     def _():
         for kind in range(2):
             halo_arrival(kind, planes - 1).wait_recv()
 
-    for copy in outs:
-        copy.wait_send()
-    first_all(2, partner, tp, lambda copy: copy.wait_send())
-    first_all(0, across_x, tx, lambda copy: copy.wait_send())
-    first_all(1, diagonal, td, lambda copy: copy.wait_send())
-
-    for src_t in (t, tp, tx, td):
-        @pl.when(src_t != z)
-        def _():
-            for j in range(W_CHUNKS):
-                for copy in second(src_t, j):
-                    copy.wait_send()
-
-    for zz in range(planes):
-        for j in range(W_CHUNKS):
-            for i in range(2):
-                third(zz, j, i).wait_send()
-        for own in range(2):
-            to_share(zz, own).wait_send()
-    for distance in range(planes):
-        for chunk in range(A_CHUNKS):
-            for way in range(2):
-                @pl.when(can_send(way, distance))
-                def _():
-                    chain(way, distance, chunk).wait_send()
-
-                if distance:
-                    @pl.when(exists(way, distance))
-                    def _():
-                        sideways(way, distance, chunk).wait_send()
-                        for far in range(2):
-                            to_partner(way, distance, chunk, far).wait_send()
-    for k in range(size - 1):
-        stat(k).wait_send()
-    for kind in range(2):
-        for r in order:
-            cross(kind, r).wait_send()
-            for far in range(2):
-                hand(kind, r, far).wait_send()
-    for distance in range(1, planes):
-        for h in range(OUT_CHUNKS):
-            for way in range(2):
-                r = z + distance if way == 0 else z - distance
-
-                @pl.when(r < planes if way == 0 else r >= 0)
-                def _():
-                    travel(way, r, h).wait_send()
+    all_sent(kv_b.at[pl.ds(0, planes * (WINDOW + 32))], halo_sem, across_y)
+    all_sent(w_all.at[pl.ds(0, 3 * block_rows)], w1_sem, partner)
+    all_sent(w_all.at[pl.ds(0, 3 * block_rows)], w2_sem, partner)
+    all_sent(w_all.at[pl.ds(0, planes * block_rows)], w3_sem, across_y)
+    all_sent(w_all.at[pl.ds(0, 2 * planes * half), pl.ds(0, width)], kc_sem, partner)
+    all_sent(rows_all.at[pl.ds(0, (planes - 1) * piece)], ax_sem, across_x)
+    all_sent(rows_all.at[pl.ds(0, 2 * (planes - 1) * piece)], ac_sem, partner)
+    all_sent(stats_all.at[pl.ds(0, size - 1)], s_sem, partner)
+
+    def sent_regions(count, sems):
+        all_sent(act.at[pl.ds(0, 2 * block), pl.ds(0, count * width // 2)], sems, partner)
+
+    @pl.when(ends)
+    def _():
+        all_sent(rows_all.at[pl.ds(0, piece)], a_sem, partner)
+        sent_regions(2 * (planes - 1), e_sem)
+        sent_regions(2, x_sem)
+        sent_regions(4, c_sem)
+        all_sent(weights.at[pl.ds(0, 4 * group)], o_sem, partner)
+
+    @pl.when(middle)
+    def _():
+        all_sent(rows_all.at[pl.ds(0, (planes + 1) * piece)], a_sem, partner)
+        sent_regions(2 * planes + 2 * (planes - 1), x_sem)
+        sent_regions(4 * planes + 4 * (planes - 1), c_sem)
+        all_sent(weights.at[pl.ds(0, 4 * group)], o_sem, partner)
+        all_sent(outgoing, r_sem, partner)
 
 
 def planned_per_device(
@@ -1077,13 +1103,13 @@
     tiles = rows // LANES
     chunks = 2 * planes * A_CHUNKS
     counts = [
-        chunks, chunks, 2 * chunks, 12, 2 * planes * W_CHUNKS, 2 * planes * W_CHUNKS, 2 * planes, 2, 3,
-        2 * planes, size, 2 * planes, 4 * planes, 2 * planes * OUT_CHUNKS,
+        chunks, chunks, 2 * planes, 3, planes * W_CHUNKS, 2 * planes, 2 * planes, 8, 1,
+        2 * planes, 1, 2 * planes, 4 * planes, 2 * planes, 3 * OUT_CHUNKS,
     ]
-    sems = [dma((n,)) for n in counts for _ in range(2)]
+    sems = [dma((n,)) for count in counts for n in (1, count)]
     return pl.pallas_call(
         functools.partial(layer_kernel, planes, CONV),
-        out_shape=jax.ShapeDtypeStruct((block, columns_out), bf16),
+        out_shape=jax.ShapeDtypeStruct((block, columns_out), f32),
         in_specs=[vmem] * 8 + [any_spec] * 5,
         out_specs=vmem,
         scratch_shapes=[
@@ -1103,14 +1129,13 @@
             pltpu.VMEM((planes + 1, 32, width), bf16),
             pltpu.VMEM((planes, 32 + block, width), f32),
             pltpu.VMEM((rows, width), f32),
-            pltpu.VMEM((rows, 2 * planes * width), bf16),
-            pltpu.VMEM((2 * planes * width, columns_out), bf16),
+            pltpu.VMEM((rows, 4 * planes * width), bf16),
+            pltpu.VMEM((4 * planes * width, columns_out), bf16),
             pltpu.VMEM((2 * tiles, LANES), f32),
             pltpu.VMEM((size, 2 * tiles, LANES), f32),
             pltpu.VMEM((2, tiles, LANES), f32),
-            pltpu.VMEM((planes, block, columns_out), bf16),
-            pltpu.VMEM((planes, block, columns_out), bf16),
-            pltpu.VMEM((planes, block, columns_out), bf16),
+            pltpu.VMEM((3, block, columns_out), bf16),
+            pltpu.VMEM((3, block, columns_out), bf16),
             dma((8,)),
         ]
         + sems,
@@ -1131,12 +1156,12 @@
         w_gate,
         out_attn,
         out_conv,
-    )
+    ).astype(bf16)
 
 
 def solution(mesh):
     planes, others = mesh.shape["tp"], mesh.shape["sp"]
-    fits = others == 2 * planes and planes % 2 == 0 and HEADS == 2 * planes * planes
+    fits = others == 2 * planes and planes == 4 and HEADS == 2 * planes * planes
     return jax.shard_map(
         planned_per_device if fits else gathered_per_device,
         mesh=mesh,

time: 152 us -> 138 us (0.908)
  Pallas kernels: 149 us -> 134 us
  other arithmetic: 0.01 us -> 2.11 us
  local copies, waits for them, and re-layouts: 2.47 us -> 0.61 us
    pallas_call x1, Pallas kernels: 149 us -> 134 us  [planned_per_device(): pl.pallas_call(functools.partial(layer_kernel, planes, CONV), out_shape=j...]
    convert_element_type x0 -> x1, other arithmetic: none -> 2.1 us  [planned_per_device(): return pl.pallas_call(functools.partial(layer_kernel, planes, CONV), out_...]
    unnamed x1 -> x0, local copies, waits for them, and re-layouts: 1.87 us -> none
where the time goes in v4:
time: 138 us; the launch traced here: 137 us
  Pallas kernels  134 us (97%)
  other arithmetic  2.11 us (2%)
    pallas_call x1, Pallas kernels, planned_per_device(): pl.pallas_call(functools.partial(layer_kernel, planes, CONV), out_shape=j...  134 us

profile of v4, /device:TPU:0, one launch (start us, length us, event | category | flops | bytes accessed | tf_op | source)
XLA Modules:
  0.0 136.8 jit_solution(15395218736331468179)
XLA Ops:
  0.0 0.6 broadcast_in_dim_tile.3.refs_2_
  0.6 134.1 %shard_map.118 = f32[256,1024]{1,0:T(8,128)} custom-call(bf16[256,4096]{1,0:T(8,128)(2,1)} %refs_0_.1, f32[1,4096]{1,0:T(1,128)} %bitcast.3, f32[1,128]{1,0:T(1,128)} %broadcast_in_dim_tile.3.refs_2_, bf16[512,128]{1,0:T(8,128)(2,1)} %refs_3_.1, bf16[512,128]{1,0:T(8,128)(2,1)} %refs_4_.1, bf16[31,512]{1,0:T(8,128)(2,1)} %refs_5_.1, f32[1,512]{1,0:T(1,128)} %bitcast.4, ...), custom_call_target="tpu_custom_call" | custom-call | tf_op jit(solution)/shard_map/pallas_call | solution.py:1110
  134.7 2.1 %convert_element_type.3 = bf16[256,1024]{1,0:T(8,128)(2,1)} convert(f32[256,1024]{1,0:T(8,128)} %shard_map.118) | non-fusion elementwise | flops 262144 | bytes 1572864 | tf_op jit(solution)/shard_map/convert_element_type | solution.py:1159
  (2 shorter events, 0.0 us)

commit v5 on v4

--- a/solution.py
+++ b/solution.py
@@ -3,6 +3,7 @@
 
 import jax
 import jax.numpy as jnp
+import numpy as np
 from jax import lax
 from jax.experimental import pallas as pl
 from jax.experimental.pallas import tpu as pltpu
@@ -263,6 +264,7 @@
 A_CHUNKS = 4
 W_CHUNKS = 4
 OUT_CHUNKS = 4
+END_CHUNKS = 4
 LANES = 128
 
 
@@ -287,14 +289,14 @@
 
 
 def layer_kernel(planes, channels, *refs):
-    (tokens, norm_gain, freq, w_key, w_value, taps, conv_gain, sink) = refs[:8]
+    (tokens_far, norm_gain, freq, w_key, w_value, taps, conv_gain, sink) = refs[:8]
     (w_query, w_glu, w_gate, out_attn, out_conv) = refs[8:13]
     mixed = refs[13]
     (rows_all, w_all, stage, w_kv, small_src, small) = refs[14:20]
     (acc, cosine, sine, q_b, kv_b, kv_rim, gated, gated_rim, extended, filtered) = refs[20:30]
-    (act, weights, stats, stats_all, moments, incoming, outgoing) = refs[30:37]
-    local_sem = refs[37]
-    pairs = [(refs[38 + 2 * i], refs[39 + 2 * i]) for i in range((len(refs) - 38) // 2)]
+    (act, weights, stats, stats_all, moments, incoming, outgoing, tokens) = refs[30:38]
+    local_sem = refs[38]
+    pairs = [(refs[39 + 2 * i], refs[40 + 2 * i]) for i in range((len(refs) - 39) // 2)]
     (a_sem, ax_sem, ac_sem, w1_sem, w2_sem, w3_sem, kc_sem, o_sem, small_sem) = pairs[:9]
     (halo_sem, s_sem, e_sem, x_sem, c_sem, r_sem) = pairs[9:15]
 
@@ -336,7 +338,12 @@
             there = pl.multiple_of(z * block + here, 16)
             rows_all[pl.ds(there, 16), :] = (value * scale * norm_gain[...]).astype(rows_all.dtype)
 
-    normalise(t * piece, piece)
+    def quarter(k):
+        part_rows = pl.ds(pl.multiple_of(lax.rem(t + k, planes) * piece, piece), piece)
+        return pltpu.make_async_copy(tokens_far.at[part_rows], tokens.at[part_rows], local_sem.at[6 + k])
+
+    for k in range(planes):
+        quarter(k).start()
 
     lane = lax.broadcasted_iota(jnp.int32, (half, 2 * HEAD), 1)
     for cc in range(2):
@@ -350,6 +357,8 @@
         small_src[tt, 0:KSIZE, :] = taps[:, cols].astype(f32)
         small_src[tt, 32:33, :] = conv_gain[:, cols]
         small_src[tt, 33:34, 0 : sink.shape[1]] = sink[...]
+    quarter(0).wait()
+    normalise(t * piece, piece)
     pl.semaphore_wait(barrier, size)
 
     def rows_of(zz, tt, chunk):
@@ -461,11 +470,12 @@
         remote(a, b, o_sem, 2 + i, at(z + ahead, y, t))
         for i, (a, b) in enumerate(zip((out_attn, out_conv), out_copies(y, 1)))
     ]
-    half_group = group // 2
+    small_group = group // END_CHUNKS
 
     def end_across(i, arrival=False):
-        start = (2 + i // 2) * part + (1 - y if arrival else y) * group + (i % 2) * half_group
-        ref = weights.at[pl.ds(pl.multiple_of(start, half_group), half_group)]
+        kind, k = i // END_CHUNKS, i % END_CHUNKS
+        start = (2 + kind) * part + (1 - y if arrival else y) * group + k * small_group
+        ref = weights.at[pl.ds(pl.multiple_of(start, small_group), small_group)]
         return remote(ref, ref, o_sem, 4 + i, across_y)
 
     outs = [
@@ -581,6 +591,7 @@
         settle(from_z, j)
 
     for k in range(1, planes):
+        quarter(k).wait()
         normalise(lax.rem(t + k, planes) * piece, piece)
     first_arrival(2)
     chain_step(1)
@@ -609,7 +620,7 @@
     @pl.when(middle)
     def _():
         end_outs[0].wait_recv()
-        for i in range(2):
+        for i in range(END_CHUNKS // 2):
             end_across(i).start()
 
     blocks_from = [
@@ -669,21 +680,20 @@
     for j in range(W_CHUNKS):
         block_step(blocks_from[2], j)
         block_step(blocks_from[3], j)
+        chain_step(planes - 1, range(j * A_CHUNKS // W_CHUNKS, (j + 1) * A_CHUNKS // W_CHUNKS))
         if j == 1:
             sideways_step(2)
         if j == 2:
-            chain_step(planes - 1, range(A_CHUNKS // 4))
             share_other((0, 1))
             for distance in range(1, planes - 1):
                 tokens_here(distance)
             multiply_own((0, 1))
             multiply_other((0, 1))
-            chain_step(planes - 1, range(A_CHUNKS // 4, A_CHUNKS // 2))
-    chain_step(planes - 1, range(A_CHUNKS // 2, A_CHUNKS))
     @pl.when(middle)
     def _():
         end_outs[1].wait_recv()
-        end_across(2).start()
+        for i in range(END_CHUNKS // 2, END_CHUNKS):
+            end_across(i).start()
 
     multiply_own((2, 3))
     share_other((2, 3))
@@ -744,7 +754,8 @@
 
     @pl.when(middle)
     def _():
-        end_across(3).start()
+        for i in range(END_CHUNKS, 2 * END_CHUNKS):
+            end_across(i).start()
 
     lane_q = lax.broadcasted_iota(jnp.int32, (WINDOW, LANES), 1)
     lane_k = lax.broadcasted_iota(jnp.int32, (2 * WINDOW, LANES), 1)
@@ -821,7 +832,7 @@
             window = extended[zz, pl.ds(base, strip + 32), :]
             total = jnp.zeros((strip, width), f32)
             for shift in range(8):
-                moved = window[shift : shift + strip + 24] if shift else window
+                moved = extended[zz, pl.ds(base + shift, strip + 24), :] if shift else window
                 for k in range((shift - 2) % 8, KSIZE, 8):
                     low = 2 + k - shift
                     total = total + moved[low : low + strip] * small[k : k + 1, :]
@@ -905,7 +916,6 @@
     @pl.when(middle)
     def _():
         pass_in(0, 0)
-        pass_in(0, 1)
 
     all_here(stats_all.at[pl.ds(0, size - 1)], s_sem, 0, partner)
     total = stats_all[0]
@@ -998,13 +1008,14 @@
 
     @pl.when(middle)
     def _():
-        for i in range(4):
+        for i in range(2 * END_CHUNKS):
             end_across(i, True).wait_recv()
 
     @pl.when(middle)
     def _():
         pass_in(1, 0)
         send_out(1, order[1])
+        pass_in(0, 1)
         gathered(0, (0, 1))
         send_sums(0, True, None, 0, across_z)
 
@@ -1094,8 +1105,8 @@
     columns_out = out_attn.shape[1]
     size = planes * planes
     half_width = HEAD // 2
-    freq = 10000.0 ** (-jnp.arange(half_width, dtype=jnp.float32) * 2.0 / HEAD)
-    freq = jnp.tile(freq, LANES // half_width)[None]
+    freq = 10000.0 ** (-np.arange(half_width, dtype=np.float64) * 2.0 / HEAD)
+    freq = jnp.asarray(np.tile(freq, LANES // half_width)[None], dtype=jnp.float32)
     vmem = pl.BlockSpec(memory_space=pltpu.VMEM)
     any_spec = pl.BlockSpec(memory_space=pl.ANY)
     dma = pltpu.SemaphoreType.DMA
@@ -1103,14 +1114,14 @@
     tiles = rows // LANES
     chunks = 2 * planes * A_CHUNKS
     counts = [
-        chunks, chunks, 2 * planes, 3, planes * W_CHUNKS, 2 * planes, 2 * planes, 8, 1,
+        chunks, chunks, 2 * planes, 3, planes * W_CHUNKS, 2 * planes, 2 * planes, 4 + 2 * END_CHUNKS, 1,
         2 * planes, 1, 2 * planes, 4 * planes, 2 * planes, 3 * OUT_CHUNKS,
     ]
     sems = [dma((n,)) for count in counts for n in (1, count)]
     return pl.pallas_call(
         functools.partial(layer_kernel, planes, CONV),
-        out_shape=jax.ShapeDtypeStruct((block, columns_out), f32),
-        in_specs=[vmem] * 8 + [any_spec] * 5,
+        out_shape=pltpu.VMEM((block, columns_out), f32),
+        in_specs=[any_spec] + [vmem] * 7 + [any_spec] * 5,
         out_specs=vmem,
         scratch_shapes=[
             pltpu.VMEM((rows, model), bf16),
@@ -1136,11 +1147,12 @@
             pltpu.VMEM((2, tiles, LANES), f32),
             pltpu.VMEM((3, block, columns_out), bf16),
             pltpu.VMEM((3, block, columns_out), bf16),
-            dma((8,)),
+            pltpu.VMEM((block, model), bf16),
+            dma((6 + planes,)),
         ]
         + sems,
         compiler_params=pltpu.CompilerParams(
-            collective_id=0, has_side_effects=True, vmem_limit_bytes=60 * 2**20
+            collective_id=0, has_side_effects=True, vmem_limit_bytes=58 * 2**20
         ),
     )(
         tokens,

time: 138 us -> 130 us (0.942)
  Pallas kernels: 134 us -> 127 us
    pallas_call x1, Pallas kernels: 134 us -> 127 us  [planned_per_device(): pl.pallas_call(functools.partial(layer_kernel, planes, CONV), out_shape=p...]
where the time goes in v5:
time: 130 us; the launch traced here: 128 us
  Pallas kernels  127 us (98%)
    pallas_call x1, Pallas kernels, planned_per_device(): pl.pallas_call(functools.partial(layer_kernel, planes, CONV), out_shape=p...  127 us

profile of v5, /device:TPU:0, one launch (start us, length us, event | category | flops | bytes accessed | tf_op | source)
XLA Modules:
  0.0 128.1 jit_solution(1030600969781487583)
XLA Ops:
  0.0 127.2 %shard_map.127 = f32[256,1024]{1,0:T(8,128)S(1)} custom-call(bf16[256,4096]{1,0:T(8,128)(2,1)} %refs_0_.1, f32[1,4096]{1,0:T(1,128)} %bitcast.3, f32[1,128]{1,0:T(1,128)} %constant.2.clone.refs_2_, bf16[512,128]{1,0:T(8,128)(2,1)} %refs_3_.1, bf16[512,128]{1,0:T(8,128)(2,1)} %refs_4_.1, bf16[31,512]{1,0:T(8,128)(2,1)} %refs_5_.1, f32[1,512]{1,0:T(1,128)} %bitcast.4, ...), custom_call_target="tpu_custom_call" | custom-call | tf_op jit(solution)/shard_map/pallas_call | solution.py:1121
  127.2 0.9 convert_element_type.3
